TPU v7x, 32 devices: a whole 2x2x4 slice. The times are simulated.
32 devices in a mesh: ep: 8 (over z, x), tp: 4 (over y, core).
Axes of the slice: x: 2, y: 2, z: 4, core: 2. Of those that a mesh axis runs over, the one named last changes fastest.
Arguments:
- query_rows: bfloat16 [4096, 3072], P('ep', 'tp'), may hold values from -6 to 6
- key_rows: bfloat16 [4096, 1024], P('ep', 'tp'), may hold values from -6 to 6
- value_rows: bfloat16 [4096, 1024], P('ep', 'tp'), may hold values from -6 to 6
- query_gain: float32 [48, 64], P('tp'), may hold values from 0.4 to 48
- key_gain: float32 [16, 64], P('tp'), may hold values from 0.1 to 1.9
- sink_logits: float32 [48], P('tp'), may hold values from 1 to 6
- out_weight: bfloat16 [3072, 2048], P('tp'), may hold values from -0.109375 to 0.109375
- expert_input: bfloat16 [4096, 2048], P(('ep', 'tp')), may hold values from -6 to 6
- expert_gain: float32 [2048], replicated, may hold values from 0.1 to 1.9
- routes: int32 [4096, 2], P(('ep', 'tp')), may hold values from 0 to 31, all different within a row; in each aligned block of 128 rows (0 to 127, 128 to 255, ...) at most 12 rows name the same one
- route_logits: float32 [4096, 2], P(('ep', 'tp')), may hold values from -6 to 6
- gate_weight: bfloat16 [32, 2048, 2048], P('ep', None, 'tp'), may hold values from -0.375 to 0.375
- up_weight: bfloat16 [32, 2048, 2048], P('ep', None, 'tp'), may hold values from -0.375 to 0.375
- down_weight: bfloat16 [32, 2048, 2048], P('ep', 'tp'), may hold values from -0.01953125 to 0.01953125
Outputs:
- attended: bfloat16 [4096, 2048], P(('ep', 'tp'))
- expert_mix: bfloat16 [4096, 2048], P(('ep', 'tp'))
Inputs may be any that keep to these rules, and one draw needn't show every extreme that they name: `routes`: each row names 2 different experts; in the rows of one device no expert is named more than 12 times, and in some device one expert is named exactly 12 times.
All inputs are finite; a program needn't handle non-finite values.
Results may differ from a plain program's by a relative error of at most 0.017.
The roundings to bfloat16 on the way count: a program that leaves them out, or rounds other values in their place, can miss the bound.
Values may be sent and summed in bfloat16 or wider, within the bound.
A program may use at most 128 MiB of HBM per device.

v0:
```python
import jax
import jax.numpy as jnp
from jax import lax
from jax.experimental import pallas as pl
from jax.experimental.pallas import tpu as pltpu
from jax.sharding import PartitionSpec as P

EXPERTS = 32
WINDOW = 128


EPSILON = 1e-06
CLAMP_LIMIT = 7.0
ACT_SLOPE = 1.702
NEGATIVE = -1e30


def shifted(value, axis, steps):
    count = lax.axis_size(axis)
    initial, last = (max(0, -steps), min(count, count - steps))
    return lax.ppermute(value, axis, [(source, source + steps) for source in range(initial, last)])


def head_norm(row_data, gain_table):
    head_count, head_size = gain_table.shape
    widened = row_data.astype(jnp.float32).reshape(row_data.shape[0], head_count, head_size)
    scaled = widened * lax.rsqrt(jnp.mean(widened * widened, axis=-1, keepdims=True) + EPSILON)
    return (scaled * gain_table).astype(jnp.bfloat16)


def band(padded, blocks):
    tiled = padded.reshape((blocks + 1, WINDOW) + padded.shape[1:])
    return jnp.concatenate([tiled[:-1], tiled[1:]], axis=1)


def attend(query_rows, key_rows, value_rows, query_gain, key_gain, sink_logits):
    seq_rows = query_rows.shape[0]
    key_heads, head_size = key_gain.shape
    group_size = query_gain.shape[0] // key_heads
    blocks = seq_rows // WINDOW
    query_hat = head_norm(query_rows, query_gain).reshape(
        blocks, WINDOW, key_heads, group_size, head_size
    )
    key_hat = head_norm(key_rows, key_gain)
    value_hat = value_rows.reshape(seq_rows, key_heads, head_size)
    tail_rows = jnp.stack([key_hat[seq_rows - WINDOW :], value_hat[seq_rows - WINDOW :]])
    earlier = shifted(tail_rows, "ep", 1)
    key_band = band(jnp.concatenate([earlier[0], key_hat], axis=0), blocks)
    value_band = band(jnp.concatenate([earlier[1], value_hat], axis=0), blocks)
    query_pos = lax.broadcasted_iota(jnp.int32, (WINDOW, 2 * WINDOW), 0)
    key_pos = lax.broadcasted_iota(jnp.int32, (WINDOW, 2 * WINDOW), 1)
    distance = query_pos + WINDOW - key_pos
    inside = (distance >= 0) & (distance < WINDOW)
    first_block = (lax.broadcasted_iota(jnp.int32, (blocks, 1, 1), 0) == 0) & (
        lax.axis_index("ep") == 0
    )
    allowed = inside[None] & ~(first_block & (key_pos < WINDOW)[None])
    scores = jnp.einsum(
        "bqkgd,bjkd->bkgqj", query_hat, key_band, preferred_element_type=jnp.float32
    ) * head_size ** (-0.5)
    scores = jnp.where(allowed[:, None, None], scores, NEGATIVE)
    sink_table = sink_logits.reshape(1, key_heads, group_size, 1, 1)
    highest = jnp.maximum(jnp.max(scores, axis=-1, keepdims=True), sink_table)
    weights = jnp.exp(scores - highest)
    total = jnp.sum(weights, axis=-1, keepdims=True) + jnp.exp(sink_table - highest)
    mixed = jnp.einsum(
        "bkgqj,bjkd->bkgqd",
        weights.astype(jnp.bfloat16),
        value_band,
        preferred_element_type=jnp.float32,
    )
    mixed = (mixed / total).astype(jnp.bfloat16)
    return jnp.transpose(mixed, (0, 3, 1, 2, 4)).reshape(seq_rows, -1)


def slot_maps(route_block, capacity):
    flat_routes = route_block.reshape(-1)
    expert_hot = (flat_routes[:, None] == lax.broadcasted_iota(jnp.int32, (1, EXPERTS), 1)).astype(
        jnp.int32
    )
    before = jnp.cumsum(expert_hot, axis=0) - expert_hot
    position = jnp.sum(before * expert_hot, axis=1)
    place_hot = (position[:, None] == lax.broadcasted_iota(jnp.int32, (1, capacity), 1)).astype(
        jnp.float32
    )
    row_total, fanout = route_block.shape
    return (
        expert_hot.astype(jnp.float32).reshape(row_total, fanout, EXPERTS),
        place_hot.reshape(row_total, fanout, capacity),
    )


def dispatch_matrix(route_block, capacity):
    expert_hot, place_hot = slot_maps(route_block, capacity)
    return jnp.einsum("rke,rkc->ecr", expert_hot, place_hot).astype(jnp.bfloat16)


def combine_matrix(route_block, route_weight, capacity):
    expert_hot, place_hot = slot_maps(route_block, capacity)
    return jnp.einsum(
        "rke,rkc,rk->rec", expert_hot, place_hot, route_weight, precision=lax.Precision.HIGHEST
    )


def expert_hidden(piece, gate_weight, up_weight):
    gate_pre = jnp.einsum("aecd,edf->aecf", piece, gate_weight, preferred_element_type=jnp.float32)
    up_pre = jnp.einsum("aecd,edf->aecf", piece, up_weight, preferred_element_type=jnp.float32)
    clipped = jnp.minimum(gate_pre, CLAMP_LIMIT)
    linear = jnp.clip(up_pre, -CLAMP_LIMIT, CLAMP_LIMIT)
    return (clipped * jax.nn.sigmoid(ACT_SLOPE * clipped) * (linear + 1.0)).astype(jnp.bfloat16)


MESH = pl.DeviceIdType.MESH


def activation(gate_pre, up_pre):
    clipped = jnp.minimum(gate_pre, CLAMP_LIMIT)
    linear = jnp.clip(up_pre, -CLAMP_LIMIT, CLAMP_LIMIT)
    return (clipped * jax.nn.sigmoid(ACT_SLOPE * clipped) * (linear + 1.0)).astype(jnp.bfloat16)


def expert_kernel(
    dims, slots, perm, unperm, gate_hbm, up_hbm, down_hbm, ret,
    gate_w, up_w, down_w, gath, xbuf, part, dbuf, sums, ybuf,
    wsem, local_sem, zs, zr, ys, yr, ds, dr, rds, rdr, rys, ryr, rzs, rzr,
):
    ep, half, local, cap, rows, width, ffn = dims
    group = 2 * half * cap
    lot = ep // 2
    me = lax.axis_index("ep")
    tp = lax.axis_index("tp")
    hi, core = tp // 2, tp % 2
    other = 1 - core
    partner = hi * 2 + other

    weights = [
        pltpu.make_async_copy(gate_hbm, gate_w, wsem.at[0]),
        pltpu.make_async_copy(up_hbm, up_w, wsem.at[1]),
        pltpu.make_async_copy(down_hbm, down_w, wsem.at[2]),
    ]
    own = pltpu.make_async_copy(slots.at[me], gath.at[me, hi, core], local_sem.at[0])
    own.start()

    barrier = pltpu.get_barrier_semaphore()
    for step in range(1, ep):
        pl.semaphore_signal(barrier, inc=1, device_id=((me + step) % ep, tp), device_id_type=MESH)
    for j in range(1, half):
        pl.semaphore_signal(
            barrier, inc=1, device_id=(me, (hi + j) % half * 2 + core), device_id_type=MESH
        )
    pl.semaphore_signal(barrier, inc=1, device_id=(me, partner), device_id_type=MESH)
    pl.semaphore_wait(barrier, ep - 1 + half - 1 + 1)

    def source(d):
        return (me - d + ep) % ep

    def z_copy(d):
        target = (me + d) % ep
        return pltpu.make_async_remote_copy(
            src_ref=slots.at[target], dst_ref=gath.at[me, hi, core],
            send_sem=zs.at[d], recv_sem=zr.at[d], device_id=(target, tp), device_id_type=MESH,
        )

    def y_copy(d, j):
        s = source(d)
        return pltpu.make_async_remote_copy(
            src_ref=gath.at[s, hi, core], dst_ref=gath.at[s, hi, core],
            send_sem=ys.at[d, j], recv_sem=yr.at[d, j],
            device_id=(me, (hi + j) % half * 2 + core), device_id_type=MESH,
        )

    def d_copy(d, j):
        s = source(d)
        block = (hi - j + half) % half
        return pltpu.make_async_remote_copy(
            src_ref=gath.at[s, block, core], dst_ref=gath.at[s, block, core],
            send_sem=ds.at[d, j], recv_sem=dr.at[d, j],
            device_id=(me, partner), device_id_type=MESH,
        )

    def rd_copy(d, h):
        s = source(d)
        return pltpu.make_async_remote_copy(
            src_ref=part.at[s, h, other], dst_ref=dbuf.at[s, h],
            send_sem=rds.at[d, h], recv_sem=rdr.at[d, h],
            device_id=(me, partner), device_id_type=MESH,
        )

    def ry_copy(d, j):
        s = source(d)
        h = (hi + j) % half
        return pltpu.make_async_remote_copy(
            src_ref=sums.at[s, h], dst_ref=ybuf.at[s, j],
            send_sem=rys.at[d, j], recv_sem=ryr.at[d, j],
            device_id=(me, h * 2 + core), device_id_type=MESH,
        )

    def rz_copy(d):
        s = source(d)
        return pltpu.make_async_remote_copy(
            src_ref=sums.at[s, hi], dst_ref=ret.at[me],
            send_sem=rzs.at[d], recv_sem=rzr.at[d], device_id=(s, tp), device_id_type=MESH,
        )

    def each(first, last, body):
        lax.fori_loop(first, last, lambda i, carry: (body(i), carry)[1], 0)

    each(1, ep, lambda d: z_copy(d).start())
    for copy in weights:
        copy.start()

    def pass_on(d):
        for j in range(1, half):
            y_copy(d, j).start()
        d_copy(d, 0).start()

    def hand_over(d):
        for j in range(1, half):
            y_copy(d, j).wait_recv()
            d_copy(d, j).start()

    def forward(d):
        z_copy(d).wait_recv()
        pass_on(d)
        hand_over(d - 1)

    own.wait()
    pass_on(0)
    each(1, lot, forward)

    tile = min(width, 512)

    def arrange(d, base):
        for j in range(half):
            d_copy(d, j).wait_recv()
        s = source(d)
        at = pl.multiple_of((d - base) * group, 16)
        for col in range(0, width, tile):
            block = gath[s, :, :, :, col : col + tile].reshape(2 * half * rows, tile)
            sorted_rows = jnp.dot(perm[...], block, preferred_element_type=jnp.float32)
            sorted_rows = sorted_rows.astype(jnp.bfloat16)
            for e in range(local):
                xbuf[e, pl.ds(at, group), col : col + tile] = sorted_rows[
                    e * group : (e + 1) * group
                ]

    def expert(e):
        x = xbuf[e]
        hidden = activation(
            jnp.dot(x, gate_w[e], preferred_element_type=jnp.float32),
            jnp.dot(x, up_w[e], preferred_element_type=jnp.float32),
        )
        for col in range(0, width, tile):
            xbuf[e, :, col : col + tile] = jnp.dot(
                hidden, down_w[e, :, col : col + tile], preferred_element_type=jnp.float32
            ).astype(jnp.bfloat16)

    def split(d, base):
        s = source(d)
        at = pl.multiple_of((d - base) * group, 16)
        for col in range(0, width, tile):
            block = jnp.concatenate(
                [xbuf[e, pl.ds(at, group), col : col + tile] for e in range(local)], axis=0
            )
            back = jnp.dot(unperm[...], block, preferred_element_type=jnp.float32)
            part[s, :, :, :, col : col + tile] = back.astype(jnp.bfloat16).reshape(
                half, 2, rows, tile
            )
        for h in range(half):
            rd_copy(d, h).start()

    def join(d):
        s = source(d)
        for h in range(half):
            rd_copy(d, h).wait_recv()
            sums[s, h] = (
                part[s, h, core].astype(jnp.float32) + dbuf[s, h].astype(jnp.float32)
            ).astype(jnp.bfloat16)
        for j in range(1, half):
            ry_copy(d, j).start()

    def finish(d):
        s = source(d)
        total = part[s, hi, core].astype(jnp.float32) + dbuf[s, hi].astype(jnp.float32)
        for j in range(1, half):
            ry_copy(d, j).wait_recv()
            total = total + ybuf[s, j].astype(jnp.float32)
        sums[s, hi] = total.astype(jnp.bfloat16)

    def give_back(d):
        finish(d)
        rz_copy(d).start()

    hand_over(lot - 1)
    each(0, lot, lambda d: arrange(d, 0))
    for copy in weights:
        copy.wait()

    share = lot // local

    def forward_late(d):
        z_copy(d).wait_recv()
        pass_on(d)

        @pl.when(d > lot)
        def _():
            hand_over(d - 1)

    def first_expert(e):
        expert(e)
        for i in range(share):
            forward_late(lot + e * share + i)

    each(0, local, first_expert)
    each(lot + local * share, ep, forward_late)

    def split_join(d, base, first):
        split(d, base)

        @pl.when(d > first)
        def _():
            join(d - 1)

    each(0, lot, lambda d: split_join(d, 0, 0))
    join(lot - 1)
    hand_over(ep - 1)
    each(lot, ep, lambda d: arrange(d, lot))

    finish(0)
    mine = pltpu.make_async_copy(sums.at[me, hi], ret.at[me], local_sem.at[1])
    mine.start()

    def give_early(d):
        @pl.when(d > 0)
        def _():
            give_back(d)

    def second_expert(e):
        expert(e)
        for i in range(share):
            give_early(e * share + i)

    each(0, local, second_expert)
    each(local * share, lot, give_early)
    each(lot, ep, lambda d: split_join(d, lot, lot))
    join(ep - 1)
    each(lot, ep, give_back)
    mine.wait()

    def drain(d):
        for j in range(1, half):
            y_copy(d, j).wait_send()
            ry_copy(d, j).wait_send()
        for j in range(half):
            d_copy(d, j).wait_send()
            rd_copy(d, j).wait_send()

    def drain_far(d):
        z_copy(d).wait_send()
        rz_copy(d).wait()

    each(0, ep, drain)
    each(1, ep, drain_far)


def run_experts(slots, dims, gate_weight, up_weight, down_weight):
    ep, half, local, cap, rows, width, ffn = dims
    tps = 2 * half
    wide = tps * rows
    order = jnp.arange(local * tps * cap)
    e, t, c = order // (tps * cap), order // cap % tps, order % cap
    perm = (t * rows + e * cap + c)[:, None] == jnp.arange(wide)[None, :]
    perm = perm.astype(jnp.bfloat16)
    dma = pltpu.SemaphoreType.DMA
    bf = jnp.bfloat16
    vm = pl.BlockSpec(memory_space=pltpu.VMEM)
    anys = pl.BlockSpec(memory_space=pl.ANY)
    copies = ep * tps * local * cap
    return pl.pallas_call(
        lambda *refs: expert_kernel(dims, *refs),
        name="expert_exchange",
        out_shape=jax.ShapeDtypeStruct((ep, rows, width), bf),
        in_specs=[vm, vm, vm, anys, anys, anys],
        out_specs=vm,
        scratch_shapes=[
            pltpu.VMEM((local, width, ffn), bf),
            pltpu.VMEM((local, width, ffn), bf),
            pltpu.VMEM((local, ffn, width), bf),
            pltpu.VMEM((ep, half, 2, rows, width), bf),
            pltpu.VMEM((local, ep // 2 * tps * cap, width), bf),
            pltpu.VMEM((ep, half, 2, rows, width), bf),
            pltpu.VMEM((ep, half, rows, width), bf),
            pltpu.VMEM((ep, half, rows, width), bf),
            pltpu.VMEM((ep, half, rows, width), bf),
            dma((3,)),
            dma((2,)),
            dma((ep,)), dma((ep,)),
            dma((ep, half)), dma((ep, half)),
            dma((ep, half)), dma((ep, half)),
            dma((ep, half)), dma((ep, half)),
            dma((ep, half)), dma((ep, half)),
            dma((ep,)), dma((ep,)),
        ],
        compiler_params=pltpu.CompilerParams(
            collective_id=0, has_side_effects=True, vmem_limit_bytes=67043328
        ),
        cost_estimate=pl.CostEstimate(
            flops=6 * copies * width * ffn, bytes_accessed=120000000, transcendentals=0
        ),
    )(slots, perm, perm.T, gate_weight, up_weight, down_weight)


def fits(dims):
    ep, half, local, cap, rows, width, ffn = dims
    if half < 1 or ep % 2 or rows % 16 or (2 * half * cap) % 16:
        return False
    held = 3 * local * width * ffn + ep * half * rows * width * 7
    held += ep * half * local * cap * width + 2 * ep * rows * width
    return 2 * held < 60 * 1024 * 1024


def slot_of(routes, cap):
    flat = routes.reshape(-1)
    hot = flat[:, None] == lax.broadcasted_iota(jnp.int32, (1, EXPERTS), 1)
    count = flat.shape[0]
    earlier = lax.broadcasted_iota(jnp.int32, (count, count), 0) > lax.broadcasted_iota(
        jnp.int32, (count, count), 1
    )
    before = jnp.dot(
        earlier.astype(jnp.bfloat16), hot.astype(jnp.bfloat16), preferred_element_type=jnp.float32
    )
    position = jnp.sum(jnp.where(hot, before, 0.0), axis=1).astype(jnp.int32)
    return (flat * cap + position).reshape(routes.shape)


def on_device(
    query_rows,
    key_rows,
    value_rows,
    query_gain,
    key_gain,
    sink_logits,
    out_weight,
    expert_input,
    expert_gain,
    routes,
    route_logits,
    gate_weight,
    up_weight,
    down_weight,
):
    heads_out = attend(query_rows, key_rows, value_rows, query_gain, key_gain, sink_logits)
    projected = jnp.dot(heads_out, out_weight, preferred_element_type=jnp.float32).astype(
        jnp.bfloat16
    )
    own_rows = expert_input.shape[0]
    fanout = routes.shape[1]
    capacity = (3 * own_rows * fanout + 2 * EXPERTS - 1) // (2 * EXPERTS)
    ep_size = lax.axis_size("ep")
    tp_size = lax.axis_size("tp")
    local_experts = gate_weight.shape[0]
    widened = expert_input.astype(jnp.float32)
    normed = (
        widened
        * lax.rsqrt(jnp.mean(widened * widened, axis=-1, keepdims=True) + EPSILON)
        * expert_gain
    ).astype(jnp.bfloat16)
    route_weight = jax.nn.softmax(route_logits, axis=-1)
    dims = (
        ep_size, tp_size // 2, local_experts, capacity, local_experts * capacity,
        expert_input.shape[1], gate_weight.shape[2],
    )
    if fits(dims):
        slot = slot_of(routes, capacity)
        places = lax.broadcasted_iota(jnp.int32, (1, EXPERTS * capacity), 1)
        sender = jnp.zeros((own_rows, EXPERTS * capacity), jnp.bool_)
        combine = jnp.zeros((own_rows, EXPERTS * capacity), jnp.float32)
        for k in range(fanout):
            taken = slot[:, k : k + 1] == places
            sender = sender | taken
            combine = combine + jnp.where(taken, route_weight[:, k : k + 1], 0.0)
        slot_rows = lax.dot_general(
            sender.astype(jnp.bfloat16), normed, (((0,), (0,)), ((), ())),
            preferred_element_type=jnp.float32,
        ).astype(jnp.bfloat16)
        slot_rows, projected = lax.optimization_barrier((slot_rows, projected))
        attended = lax.psum_scatter(projected, "tp", scatter_dimension=0, tiled=True)
        returned = run_experts(
            slot_rows.reshape(ep_size, local_experts * capacity, -1), dims,
            gate_weight, up_weight, down_weight,
        ).reshape(EXPERTS * capacity, -1)
        expert_mix = jnp.dot(
            combine, returned.astype(jnp.float32), precision=lax.Precision.HIGHEST
        ).astype(jnp.bfloat16)
    else:
        attended = lax.psum_scatter(projected, "tp", scatter_dimension=0, tiled=True)
        combine = combine_matrix(routes, route_weight, capacity)
        sender = dispatch_matrix(routes, capacity)
        slot_rows = jnp.einsum(
            "ecr,rd->ecd", sender, normed, preferred_element_type=jnp.float32
        ).astype(jnp.bfloat16)
        slot_rows = slot_rows.reshape(ep_size, local_experts, capacity, -1)
        arrived = lax.all_to_all(slot_rows, "ep", split_axis=0, concat_axis=0, tiled=True)
        hidden_units = expert_hidden(
            lax.all_gather(arrived, "tp", axis=0, tiled=True), gate_weight, up_weight
        )
        partial_value = jnp.einsum(
            "aecf,efd->aecd", hidden_units, down_weight, preferred_element_type=jnp.float32
        ).astype(jnp.bfloat16)
        partial_value = partial_value.reshape(tp_size, ep_size * local_experts * capacity, -1)
        pieces = lax.all_to_all(partial_value, "tp", split_axis=0, concat_axis=0, tiled=True)
        summed = jnp.sum(pieces, axis=0, dtype=jnp.float32).astype(jnp.bfloat16)
        summed = summed.reshape(ep_size, local_experts * capacity, -1)
        returned = lax.all_to_all(summed, "ep", split_axis=0, concat_axis=0, tiled=True).reshape(
            EXPERTS, capacity, -1
        )
        expert_mix = jnp.einsum(
            "rec,ecd->rd", combine, returned.astype(jnp.float32), precision=lax.Precision.HIGHEST
        ).astype(jnp.bfloat16)
    return (attended, expert_mix)


def solution(mesh):
    placed = (
        P("ep", "tp"),
        P("ep", "tp"),
        P("ep", "tp"),
        P("tp", None),
        P("tp", None),
        P("tp"),
        P("tp", None),
        P(("ep", "tp"), None),
        P(),
        P(("ep", "tp"), None),
        P(("ep", "tp"), None),
        P("ep", None, "tp"),
        P("ep", None, "tp"),
        P("ep", "tp", None),
    )
    return jax.shard_map(
        on_device,
        mesh=mesh,
        in_specs=placed,
        out_specs=(P(("ep", "tp"), None), P(("ep", "tp"), None)),
        check_vma=False,
    )
```

profile of v0, /device:TPU:0, one launch (start us, length us, event | category | flops | bytes accessed | tf_op | source)
XLA Modules:
  0.0 162.8 jit_solution(3600350288417380128)
XLA Ops:
  7.2 1.2 copy.50
  8.5 0.8 multiply_convert_fusion.1
  9.3 0.7 copy-done.2
  10.0 1.1 copy.51
  11.1 0.7 pad_maximum_fusion.2
  11.8 5.5 %collective-permute-start = (bf16[2,128,4,64]{1,3,2,0:T(8,128)(2,1)}, bf16[2,128,4,64]{1,3,2,0:T(8,128)(2,1)}, u32[]{:S(2)}, u32[]{:S(2)}) collective-permute-start(bf16[2,128,4,64]{1,3,2,0:T(8,128)(2,1)} %pad_maximum_fusion.2), channel_id=1, source_target_pairs={{0,4},{4,8},{8,12},{12,16},{16,20},{20,24},{24,28},{1,5},{5,9},{9,... | collective-permute-start | bytes 393224 | tf_op jit(solution)/shard_map/ppermute | solution.py:21
  17.3 0.2 reshape.176
  17.5 0.3 copy.54
  17.8 1.4 convert_multiply_fusion.2
  19.2 0.5 reshape.177
  19.7 1.2 reshape.184
  21.0 1.6 reduce_sum.57
  22.8 0.3 copy.59
  23.1 0.1 copy.48
  23.2 0.1 eq.79
  23.4 0.2 fusion.12
  23.6 0.1 convert_element_type.55
  23.9 0.2 fusion.13
  24.1 0.1 fusion.26
  24.2 1.2 multiply_convert_fusion
  25.4 1.8 %convolution_convert_fusion.1 = bf16[384,2048]{1,0:T(8,128)(2,1)} fusion(bf16[128,2048]{1,0:T(8,128)(2,1)S(1)} %copy-done.1, f32[2048]{0:T(1024)S(1)} %copy-done.8, f32[128]{0:T(128)S(1)} %add_rsqrt_fusion.2, s32[128]{0:T(128)S(1)} %get-tuple-element.15, s32[128]{0:T(128)S(1)} %get-tuple-element.14), kind=kOutput, calls=%fused_computation.11 | convolution fusion | flops 203309056 | bytes 2106880 | tf_op jit(solution)/shard_map/dot_general | solution.py:482
  27.2 0.2 not_and_fusion
  27.4 0.9 slice_bitcast_fusion.1
  28.5 1.1 fusion.2
  29.7 1.6 fusion
  31.5 1.6 fusion.9
  33.1 0.6 copy.61
  33.7 3.2 %convolution_convert_fusion = bf16[512,2048]{1,0:T(8,128)(2,1)} fusion(bf16[768,2048]{1,0:T(8,128)(2,1)S(1)} %copy-done, bf16[96,8,4,128]{3,2,1,0:T(4,128)(2,1)S(1)} %bitcast.79), kind=kOutput, calls=%fused_computation.10 | convolution fusion | flops 1611661312 | bytes 6029312 | tf_op jit(solution)/shard_map/dot_general | solution.py:453
  37.1 0.6 slice_bitcast_fusion.4
  37.7 0.7 fusion.37
  38.4 114.3 %expert_exchange.1 = bf16[8,48,2048]{2,1,0:T(8,128)(2,1)} custom-call(bf16[8,48,2048]{2,1,0:T(8,128)(2,1)} %bitcast.81, bf16[192,192]{1,0:T(8,128)(2,1)} %get-tuple-element.13.refs_1_, bf16[192,192]{1,0:T(8,128)(2,1)} %get-tuple-element.12.refs_2_, bf16[4,2048,512]{2,1,0:T(8,128)(2,1)} %refs_3_.1, bf16[4,2048,512]{2,1,0:T(8,128)(2,1)} %refs_4_.1, ...), custom_call_target="tpu_custom_call" | custom-call | flops 9663676416 | bytes 120000000 | tf_op jit(solution)/shard_map/expert_exchange/pallas_call | solution.py:379
  152.7 3.3 %convolution_convert_fusion.2 = bf16[128,2048]{1,0:T(8,128)(2,1)} fusion(bf16[384,2048]{1,0:T(8,128)(2,1)} %bitcast.80, f32[128]{0:T(128)} %get-tuple-element.11, f32[128]{0:T(128)} %get-tuple-element.10, s32[128]{0:T(128)} %copy-done.12, s32[128]{0:T(128)} %copy-done.11), kind=kOutput, calls=%fused_computation.12 | convolution fusion | flops 1208467456 | bytes 2099200 | tf_op jit(solution)/shard_map/dot_general | solution.py:492
  (59 shorter events, 0.9 us)
Async XLA Ops:
  7.2 10.3 %copy-start.6 = (bf16[512,768]{1,0:T(8,128)(2,1)S(1)}, bf16[512,768]{1,0:T(8,128)(2,1)}, u32[]{:S(2)}) copy-start(bf16[512,768]{1,0:T(8,128)(2,1)} %param.14) | copy-start | bytes 2359300
  7.2 148.8 %reduce-scatter.2.cloned.1.call-start = ((), (), s32[]{:S(2)}) async-start(), calls=%async_computation.1 | async-start | bytes 2621440 | tf_op jit(solution)/shard_map/reduce_scatter | solution.py:487
  9.3 0.7 copy-start.2
  11.1 6.7 %copy-start.4 = (bf16[512,256]{0,1:T(8,128)(2,1)}, bf16[512,256]{0,1:T(8,128)(2,1)S(1)}, u32[]{:S(2)}) copy-start(bf16[512,256]{0,1:T(8,128)(2,1)S(1)} %copy.51) | copy-start | bytes 786436
  11.8 15.6 %collective-permute-start = (bf16[2,128,4,64]{1,3,2,0:T(8,128)(2,1)}, bf16[2,128,4,64]{1,3,2,0:T(8,128)(2,1)}, u32[]{:S(2)}, u32[]{:S(2)}) collective-permute-start(bf16[2,128,4,64]{1,3,2,0:T(8,128)(2,1)} %pad_maximum_fusion.2), channel_id=1, source_target_pairs={{0,4},{4,8},{8,12},{12,16},{16,20},{20,24},{24,28},{1,5},{5,9},{9,... | collective-permute-start | bytes 393224 | tf_op jit(solution)/shard_map/ppermute | solution.py:21
  17.8 4.8 %copy-start.10 = (f32[12,64]{1,0:T(8,128)S(1)}, f32[12,64]{1,0:T(8,128)}, u32[]{:S(2)}) copy-start(f32[12,64]{1,0:T(8,128)} %param.17) | copy-start | bytes 9220
  17.8 4.9 %copy-start.14 = (f32[12]{0:T(128)S(1)}, f32[12]{0:T(128)}, u32[]{:S(2)}) copy-start(f32[12]{0:T(128)} %param.19) | copy-start | bytes 148
  19.2 3.9 %copy-start.13 = (s32[128,2]{0,1:T(2,128)S(1)}, s32[128,2]{0,1:T(2,128)}, u32[]{:S(2)}) copy-start(s32[128,2]{0,1:T(2,128)} %param.23) | copy-start | bytes 3076
  19.2 4.6 %copy-start.1 = (bf16[128,2048]{1,0:T(8,128)(2,1)S(1)}, bf16[128,2048]{1,0:T(8,128)(2,1)}, u32[]{:S(2)}) copy-start(bf16[128,2048]{1,0:T(8,128)(2,1)} %param.21) | copy-start | bytes 1572868
  19.2 4.8 %copy-start.9 = (f32[4,64]{1,0:T(4,128)S(1)}, f32[4,64]{1,0:T(4,128)}, u32[]{:S(2)}) copy-start(f32[4,64]{1,0:T(4,128)} %param.18) | copy-start | bytes 3076
  21.0 4.4 %copy-start.8 = (f32[2048]{0:T(1024)S(1)}, f32[2048]{0:T(1024)}, u32[]{:S(2)}) copy-start(f32[2048]{0:T(1024)} %param.22) | copy-start | bytes 24580
  23.8 4.5 %copy-start.3 = (bf16[512,4,64]{0,2,1:T(8,128)(2,1)S(1)}, bf16[512,4,64]{0,2,1:T(8,128)(2,1)}, u32[]{:S(2)}) copy-start(bf16[512,4,64]{0,2,1:T(8,128)(2,1)} %copy-done.2) | copy-start | bytes 786436
  23.8 4.5 %copy-start.5 = (bf16[512,256]{0,1:T(8,128)(2,1)S(1)}, bf16[512,256]{0,1:T(8,128)(2,1)}, u32[]{:S(2)}) copy-start(bf16[512,256]{0,1:T(8,128)(2,1)} %copy-done.4) | copy-start | bytes 786436
  23.8 3.5 %copy-start.11 = (s32[128]{0:T(128)}, s32[128]{0:T(128)S(1)}, u32[]{:S(2)}) copy-start(s32[128]{0:T(128)S(1)} %get-tuple-element.14) | copy-start | bytes 1540
  23.9 3.5 %copy-start.12 = (s32[128]{0:T(128)}, s32[128]{0:T(128)S(1)}, u32[]{:S(2)}) copy-start(s32[128]{0:T(128)S(1)} %get-tuple-element.15) | copy-start | bytes 1540
  31.4 2.3 %copy-start = (bf16[768,2048]{1,0:T(8,128)(2,1)S(1)}, bf16[768,2048]{1,0:T(8,128)(2,1)}, u32[]{:S(2)}) copy-start(bf16[768,2048]{1,0:T(8,128)(2,1)} %param.20) | copy-start | bytes 9437188
  33.7 3.3 %copy-start.7 = (f32[128,2]{0,1:T(2,128)S(1)}, f32[128,2]{0,1:T(2,128)}, u32[]{:S(2)}) copy-start(f32[128,2]{0,1:T(2,128)} %param.24) | copy-start | bytes 3076
Sparse Core Ops, SparseCore 0:
  37.1 35.9 reduce-scatter.1
where the time goes:
time: 163 us
  Pallas kernels  114 us (70%)
  between operations  14.5 us (9%)
  matrix products  11.3 us (7%)
  other arithmetic  8.93 us (5%)
  local copies, waits for them, and re-layouts  8.25 us (5%)
  starting transfers between devices  5.55 us (3%)
    pallas_call x1, Pallas kernels, run_experts(): pl.pallas_call(lambda *refs: expert_kernel(dims, *refs), name='expert_exc...  114 us
    ppermute x1, starting transfers between devices, shifted(): lax.ppermute(value, axis, [(source, source + steps) for source in range(i...  5.52 us
    unnamed x34, local copies, waits for them, and re-layouts  3.4 us
    dot_general x1, matrix products, on_device(): jnp.dot(combine, returned.astype(jnp.float32), precision=lax.Precision.HI...  3.26 us
  transfers between devices with their start and end apart: 2, of which 0 were waited for; matrix products, arithmetic and copies ran while one was open for 9% of the time, Pallas kernels for 70%

commit v1 on v0

v1 whole, which is shorter than its diff:
```python
import jax
import jax.numpy as jnp
import numpy as np
from jax import lax
from jax.experimental import pallas as pl
from jax.experimental.pallas import tpu as pltpu
from jax.sharding import PartitionSpec as P

EXPERTS = 32
WINDOW = 128


EPSILON = 1e-06
CLAMP_LIMIT = 7.0
ACT_SLOPE = 1.702
NEGATIVE = -1e30


def shifted(value, axis, steps):
    count = lax.axis_size(axis)
    initial, last = (max(0, -steps), min(count, count - steps))
    return lax.ppermute(value, axis, [(source, source + steps) for source in range(initial, last)])


def head_norm(row_data, gain_table):
    head_count, head_size = gain_table.shape
    widened = row_data.astype(jnp.float32).reshape(row_data.shape[0], head_count, head_size)
    scaled = widened * lax.rsqrt(jnp.mean(widened * widened, axis=-1, keepdims=True) + EPSILON)
    return (scaled * gain_table).astype(jnp.bfloat16)


def band(padded, blocks):
    tiled = padded.reshape((blocks + 1, WINDOW) + padded.shape[1:])
    return jnp.concatenate([tiled[:-1], tiled[1:]], axis=1)


def attend(query_rows, key_rows, value_rows, query_gain, key_gain, sink_logits):
    seq_rows = query_rows.shape[0]
    key_heads, head_size = key_gain.shape
    group_size = query_gain.shape[0] // key_heads
    blocks = seq_rows // WINDOW
    query_hat = head_norm(query_rows, query_gain).reshape(
        blocks, WINDOW, key_heads, group_size, head_size
    )
    key_hat = head_norm(key_rows, key_gain)
    value_hat = value_rows.reshape(seq_rows, key_heads, head_size)
    tail_rows = jnp.stack([key_hat[seq_rows - WINDOW :], value_hat[seq_rows - WINDOW :]])
    earlier = shifted(tail_rows, "ep", 1)
    key_band = band(jnp.concatenate([earlier[0], key_hat], axis=0), blocks)
    value_band = band(jnp.concatenate([earlier[1], value_hat], axis=0), blocks)
    query_pos = lax.broadcasted_iota(jnp.int32, (WINDOW, 2 * WINDOW), 0)
    key_pos = lax.broadcasted_iota(jnp.int32, (WINDOW, 2 * WINDOW), 1)
    distance = query_pos + WINDOW - key_pos
    inside = (distance >= 0) & (distance < WINDOW)
    first_block = (lax.broadcasted_iota(jnp.int32, (blocks, 1, 1), 0) == 0) & (
        lax.axis_index("ep") == 0
    )
    allowed = inside[None] & ~(first_block & (key_pos < WINDOW)[None])
    scores = jnp.einsum(
        "bqkgd,bjkd->bkgqj", query_hat, key_band, preferred_element_type=jnp.float32
    ) * head_size ** (-0.5)
    scores = jnp.where(allowed[:, None, None], scores, NEGATIVE)
    sink_table = sink_logits.reshape(1, key_heads, group_size, 1, 1)
    highest = jnp.maximum(jnp.max(scores, axis=-1, keepdims=True), sink_table)
    weights = jnp.exp(scores - highest)
    total = jnp.sum(weights, axis=-1, keepdims=True) + jnp.exp(sink_table - highest)
    mixed = jnp.einsum(
        "bkgqj,bjkd->bkgqd",
        weights.astype(jnp.bfloat16),
        value_band,
        preferred_element_type=jnp.float32,
    )
    mixed = (mixed / total).astype(jnp.bfloat16)
    return jnp.transpose(mixed, (0, 3, 1, 2, 4)).reshape(seq_rows, -1)


def slot_maps(route_block, capacity):
    flat_routes = route_block.reshape(-1)
    expert_hot = (flat_routes[:, None] == lax.broadcasted_iota(jnp.int32, (1, EXPERTS), 1)).astype(
        jnp.int32
    )
    before = jnp.cumsum(expert_hot, axis=0) - expert_hot
    position = jnp.sum(before * expert_hot, axis=1)
    place_hot = (position[:, None] == lax.broadcasted_iota(jnp.int32, (1, capacity), 1)).astype(
        jnp.float32
    )
    row_total, fanout = route_block.shape
    return (
        expert_hot.astype(jnp.float32).reshape(row_total, fanout, EXPERTS),
        place_hot.reshape(row_total, fanout, capacity),
    )


def dispatch_matrix(route_block, capacity):
    expert_hot, place_hot = slot_maps(route_block, capacity)
    return jnp.einsum("rke,rkc->ecr", expert_hot, place_hot).astype(jnp.bfloat16)


def combine_matrix(route_block, route_weight, capacity):
    expert_hot, place_hot = slot_maps(route_block, capacity)
    return jnp.einsum(
        "rke,rkc,rk->rec", expert_hot, place_hot, route_weight, precision=lax.Precision.HIGHEST
    )


def expert_hidden(piece, gate_weight, up_weight):
    gate_pre = jnp.einsum("aecd,edf->aecf", piece, gate_weight, preferred_element_type=jnp.float32)
    up_pre = jnp.einsum("aecd,edf->aecf", piece, up_weight, preferred_element_type=jnp.float32)
    clipped = jnp.minimum(gate_pre, CLAMP_LIMIT)
    linear = jnp.clip(up_pre, -CLAMP_LIMIT, CLAMP_LIMIT)
    return (clipped * jax.nn.sigmoid(ACT_SLOPE * clipped) * (linear + 1.0)).astype(jnp.bfloat16)


MESH = pl.DeviceIdType.MESH
BF = jnp.bfloat16
F32 = jnp.float32


def dot(left, right):
    return jnp.dot(left, right, preferred_element_type=F32)


def activation(gate_pre, up_pre):
    clipped = jnp.minimum(gate_pre, CLAMP_LIMIT)
    linear = jnp.clip(up_pre, -CLAMP_LIMIT, CLAMP_LIMIT)
    return (clipped * jax.nn.sigmoid(ACT_SLOPE * clipped) * (linear + 1.0)).astype(BF)


def iota(shape, axis):
    return lax.broadcasted_iota(jnp.int32, shape, axis)


def fused_kernel(
    dims, tok, gain, info, sink, qgain, kgain, perm, unperm,
    q_hbm, k_hbm, v_hbm, wo_hbm, gate_hbm, up_hbm, down_hbm,
    attended, mixed,
    gate_w, up_w, down_w, wo, qbuf, kext, vext, kd, vd, ho,
    slots, nslots, ntok, ninfo, nrm, gath, xbuf, dbuf, sums, ybuf, retn, retx,
    nsend, nrecv, pbuf, abuf, asend, arecv,
    lsem, zs, zr, ns, nr, ys, yr, ds, dr, rds, rdr, rys, ryr, rzs, rzr, ms, mr,
):
    ep, local, cap, rows, width, ffn, own, seq, kv_heads, q_heads, experts = dims
    lot = ep // 2
    group = 4 * cap
    sorted_rows = 4 * rows
    tile = 512
    pairs = q_heads // 2
    me = lax.axis_index("ep")
    tp = lax.axis_index("tp")
    hi, core = tp // 2, tp % 2
    other = 1 - core
    partner = (me, hi * 2 + other)
    across = (me, (1 - hi) * 2 + core)

    def mate(d):
        found, bit = me, 1
        while bit < ep:
            if d & bit:
                found = found + bit - 2 * bit * (me // bit % 2)
            bit *= 2
        return found

    def remote(src, dst, send, recv, device):
        return pltpu.make_async_remote_copy(
            src_ref=src, dst_ref=dst, send_sem=send, recv_sem=recv,
            device_id=device, device_id_type=MESH,
        )

    halo = WINDOW
    k_in = pltpu.make_async_copy(k_hbm, kext.at[pl.ds(halo, seq)], lsem.at[0])
    v_in = pltpu.make_async_copy(v_hbm, vext.at[pl.ds(halo, seq)], lsem.at[1])
    q_in = pltpu.make_async_copy(q_hbm, qbuf, lsem.at[2])
    wo_in = pltpu.make_async_copy(wo_hbm, wo, lsem.at[3])
    weights = [
        pltpu.make_async_copy(gate_hbm, gate_w, lsem.at[4]),
        pltpu.make_async_copy(up_hbm, up_w, lsem.at[5]),
        pltpu.make_async_copy(down_hbm, down_w, lsem.at[6]),
    ]

    info_y = remote(info, ninfo, ms.at[0], mr.at[0], across)
    tok_y = remote(tok, ntok, ms.at[1], mr.at[1], across)
    following = ((me + 1) % ep, tp)
    k_halo = remote(
        k_hbm.at[pl.ds(seq - halo, halo)], kext.at[pl.ds(0, halo)], ms.at[2], mr.at[2], following
    )
    v_halo = remote(
        v_hbm.at[pl.ds(seq - halo, halo)], vext.at[pl.ds(0, halo)], ms.at[3], mr.at[3], following
    )
    att_d = remote(pbuf.at[other], abuf, ms.at[4], mr.at[4], partner)
    pieces = 4
    piece = own // pieces

    def att_y(i):
        at = pl.ds(i * piece, piece)
        return remote(asend.at[at], arecv.at[at], ms.at[6 + i], mr.at[6 + i], across)

    def mix_y(i):
        at = pl.ds(i * (own // 2), own // 2)
        return remote(nsend.at[at], nrecv.at[at], ms.at[10 + i], mr.at[10 + i], across)

    def z_copy(d):
        return remote(slots.at[d], gath.at[d, core, hi], zs.at[d], zr.at[d], (mate(d), tp))

    def n_copy(d):
        return remote(nslots.at[d], gath.at[d, core, 1 - hi], ns.at[d], nr.at[d], (mate(d), tp))

    def y_copy(d):
        block = gath.at[d, core, hi]
        return remote(block, block, ys.at[d - lot], yr.at[d - lot], across)

    def d_copy(d):
        block = gath.at[d, core]
        return remote(block, block, ds.at[d], dr.at[d], partner)

    def rd_copy(d):
        return remote(gath.at[d, other], dbuf.at[d], rds.at[d], rdr.at[d], partner)

    def ry_copy(d):
        return remote(
            sums.at[d, 1 - hi], ybuf.at[d - lot], rys.at[d - lot], ryr.at[d - lot], across
        )

    def rz_copy(d):
        if d < lot:
            return remote(sums.at[d], retn.at[:, d], rzs.at[d], rzr.at[d], (mate(d), tp))
        return remote(sums.at[d, hi], retx.at[d - lot], rzs.at[d], rzr.at[d], (mate(d), tp))

    def placed(table):
        expert_ids = iota((experts, own), 0).astype(F32)
        hot = [(table[k : k + 1] == expert_ids).astype(F32) for k in range(2)]
        earlier = (iota((own, own), 0) < iota((own, own), 1)).astype(BF)
        before = dot((hot[0] + hot[1]).astype(BF), earlier)
        slot = [
            table[k : k + 1] * cap + jnp.sum(before * hot[k], axis=0, keepdims=True)
            for k in range(2)
        ]
        top = jnp.maximum(table[2:3], table[3:4])
        raised = [jnp.exp(table[2 + k : 3 + k] - top) for k in range(2)]
        share = [raised[k] / (raised[0] + raised[1]) for k in range(2)]
        return slot, share

    def wanted(first, last, axis):
        count = (last - first) * rows
        shape = (count, 1) if axis == 0 else (1, count)
        place = iota(shape, axis)
        found = place
        for d in range(first, last):
            inside = (place >= (d - first) * rows) & (place < (d - first + 1) * rows)
            found = found + jnp.where(inside, (mate(d) - (d - first)) * rows, 0)
        return found.astype(F32)

    def picker(slot, first, last):
        target = wanted(first, last, 0)
        return ((slot[0] == target) | (slot[1] == target)).astype(BF)

    def column(row):
        diagonal = iota((own, own), 0) == iota((own, own), 1)
        return jnp.sum(jnp.where(diagonal, row, 0.0), axis=1, keepdims=True)

    def combiner(slot, share, first, last):
        target = wanted(first, last, 1)
        full = jnp.where(column(slot[0]) == target, column(share[0]), 0.0)
        full = full + jnp.where(column(slot[1]) == target, column(share[1]), 0.0)
        high = full.astype(BF)
        return high, (full - high.astype(F32)).astype(BF)

    def normalise(source):
        wide = source[...].astype(F32)
        mean = jnp.mean(wide * wide, axis=-1, keepdims=True)
        nrm[...] = (wide * lax.rsqrt(mean + EPSILON) * gain[...]).astype(BF)

    for copy in (k_in, v_in, q_in, wo_in):
        copy.start()
    barrier = pltpu.get_barrier_semaphore()
    for d in range(1, ep):
        pl.semaphore_signal(barrier, inc=1, device_id=(mate(d), tp), device_id_type=MESH)
    pl.semaphore_signal(barrier, inc=1, device_id=across, device_id_type=MESH)
    pl.semaphore_signal(barrier, inc=1, device_id=partner, device_id_type=MESH)

    own_slot, own_share = placed(info[...])
    normalise(tok)
    own_pick = picker(own_slot, 0, ep)
    for col in range(0, width, tile):
        picked = dot(own_pick, nrm[:, col : col + tile]).astype(BF)
        slots[:, :, col : col + tile] = picked.reshape(ep, rows, tile)
        gath[0, core, hi, :, col : col + tile] = picked[:rows]

    pl.semaphore_wait(barrier, ep + 1)
    info_y.start()
    tok_y.start()

    @pl.when(me < ep - 1)
    def _():
        k_halo.start()
        v_halo.start()

    for d in list(range(lot, ep)) + list(range(1, lot)):
        z_copy(d).start()
    for copy in weights:
        copy.start()

    low_half = iota((1, 128), 1) < 64
    same_head = (iota((128, 128), 0) // 64 == iota((128, 128), 1) // 64).astype(BF)

    def head_scaled(block, gain_row):
        wide = block.astype(F32)
        square = wide * wide
        high = square.astype(BF)
        rest = (square - high.astype(F32)).astype(BF)
        mean = (dot(high, same_head) + dot(rest, same_head)) * (1.0 / 64.0)
        return wide * lax.rsqrt(mean + EPSILON) * gain_row

    def spread(values, target, m, start, count):
        turned = pltpu.roll(values, 64, 1)
        target[2 * m, pl.ds(start, count)] = jnp.where(low_half, values, turned).astype(BF)
        target[2 * m + 1, pl.ds(start, count)] = jnp.where(low_half, turned, values).astype(BF)

    def prepare(start, count):
        for m in range(kv_heads // 2):
            cols = slice(m * 128, (m + 1) * 128)
            keys = head_scaled(kext[pl.ds(start, count), cols], kgain[m : m + 1])
            spread(keys.astype(BF).astype(F32), kd, m, start, count)
            spread(vext[pl.ds(start, count), cols].astype(F32), vd, m, start, count)

    share_heads = q_heads // kv_heads

    def attend_pair(b, m):
        top_row = pl.multiple_of(b * WINDOW, WINDOW)
        tiles = share_heads
        low_key = jnp.where((b == 0) & (me == 0), WINDOW, 0)
        query = iota((WINDOW, 2 * WINDOW), 0)
        key = iota((WINDOW, 2 * WINDOW), 1)
        allowed = (key > query) & (key <= query + WINDOW) & (key >= low_key)
        for j in range(tiles):
            lane = pl.multiple_of((m * tiles + j) * 128, 128)
            scaled = head_scaled(
                qbuf[pl.ds(top_row, WINDOW), pl.ds(lane, 128)], qgain[pl.ds(m * tiles + j, 1)]
            ).astype(BF).astype(F32) * 0.125
            outs = []
            for half in range(2):
                head = 2 * j + half
                kv = 2 * m + head // share_heads
                mask = low_half if half == 0 else jnp.logical_not(low_half)
                query_hat = jnp.where(mask, scaled, 0.0).astype(BF)
                keys = kd[kv, pl.ds(top_row, 2 * WINDOW)]
                scores = lax.dot_general(
                    query_hat, keys, (((1,), (1,)), ((), ())), preferred_element_type=F32
                )
                scores = jnp.where(allowed, scores, NEGATIVE)
                sink_value = sink[0, 2 * tiles * m + head]
                highest = jnp.maximum(jnp.max(scores, axis=-1, keepdims=True), sink_value)
                raised = jnp.exp(scores - highest)
                total = jnp.sum(raised, axis=-1, keepdims=True) + jnp.exp(sink_value - highest)
                product = dot(raised.astype(BF), vd[kv, pl.ds(top_row, 2 * WINDOW)])
                outs.append(product / total)
            ho[pl.ds(top_row, WINDOW), pl.ds(lane, 128)] = jnp.where(
                low_half, outs[0], outs[1]
            ).astype(BF)

    k_in.wait()
    v_in.wait()

    @pl.when(me == 0)
    def _():
        kext[0:halo] = jnp.zeros((halo, kext.shape[1]), BF)
        vext[0:halo] = jnp.zeros((halo, vext.shape[1]), BF)

    prepare(halo, seq)
    q_in.wait()
    blocks = seq // WINDOW

    def attend_block(i, carry):
        b = (i + 1) % blocks

        @pl.when(i == blocks - 1)
        def _():
            @pl.when(me > 0)
            def _():
                k_halo.wait_recv()
                v_halo.wait_recv()

            prepare(0, halo)

        lax.fori_loop(0, kv_heads // 2, lambda m, c: (attend_pair(b, m), c)[1], 0)
        return carry

    def forward(d):
        z_copy(d).wait_recv()
        y_copy(d).start()

    lax.fori_loop(0, blocks, attend_block, 0)
    forward(lot)
    wo_in.wait()

    def project(i, carry):
        lane = pl.ds(pl.multiple_of(i * 256, 256), 256)
        result = dot(ho[...], wo[:, lane]).astype(BF)
        for t in range(4):
            pbuf[t % 2, t // 2, :, lane] = result[t * own : (t + 1) * own]
        return carry

    lax.fori_loop(0, width // 256, project, 0)
    att_d.start()

    info_y.wait_recv()
    tok_y.wait_recv()
    next_slot, next_share = placed(ninfo[...])
    normalise(ntok)
    next_pick = picker(next_slot, 0, lot)
    for col in range(0, width, tile):
        picked = dot(next_pick, nrm[:, col : col + tile]).astype(BF)
        nslots[:, :, col : col + tile] = picked.reshape(lot, rows, tile)
        gath[0, core, 1 - hi, :, col : col + tile] = picked[:rows]
    for d in range(1, lot):
        n_copy(d).start()
    d_copy(0).start()

    att_d.wait_recv()
    asend[...] = (pbuf[core, 1 - hi].astype(F32) + abuf[1 - hi].astype(F32)).astype(BF)

    def arrange(d, at):
        d_copy(d).wait_recv()
        for col in range(0, width, tile):
            block = gath[d, :, :, :, col : col + tile].reshape(sorted_rows, tile)
            moved = dot(perm[...], block).astype(BF)
            for e in range(local):
                xbuf[e, at : at + group, col : col + tile] = moved[e * group : (e + 1) * group]

    def run(count):
        def expert(e, carry):
            x = xbuf[e, 0:count]
            hidden = activation(dot(x, gate_w[e]), dot(x, up_w[e]))
            for col in range(0, width, tile):
                xbuf[e, 0:count, col : col + tile] = dot(
                    hidden, down_w[e, :, col : col + tile]
                ).astype(BF)
            return carry

        lax.fori_loop(0, local, expert, 0)

    def split(d, at):
        d_copy(d).wait_send()
        if d >= lot:
            y_copy(d).wait_send()
        for col in range(0, width, tile):
            block = jnp.concatenate(
                [xbuf[e, at : at + group, col : col + tile] for e in range(local)], axis=0
            )
            back = dot(unperm[...], block).astype(BF)
            gath[d, :, :, :, col : col + tile] = back.reshape(2, 2, rows, tile)
        rd_copy(d).start()

    def join(d):
        rd_copy(d).wait_recv()
        if d >= lot:
            part = gath[d, core, 1 - hi].astype(F32) + dbuf[d, 1 - hi].astype(F32)
            sums[d, 1 - hi] = part.astype(BF)
            ry_copy(d).start()
            return
        for h in range(2):
            part = (gath[d, core, h].astype(F32) + dbuf[d, h].astype(F32)).astype(BF)
            if d == 0:
                retn[h, 0] = part
            else:
                sums[d, h] = part
        if d > 0:
            rz_copy(d).start()

    def finish(d):
        ry_copy(d).wait_recv()
        total = gath[d, core, hi].astype(F32) + dbuf[d, hi].astype(F32)
        sums[d, hi] = (total + ybuf[d - lot].astype(F32)).astype(BF)
        rz_copy(d).start()

    def hand_over(d):
        if d >= lot:
            y_copy(d).wait_recv()
        elif d > 0:
            z_copy(d).wait_recv()
            n_copy(d).wait_recv()
        if d > 0:
            d_copy(d).start()

    def crossing(d):
        arrange(d, 0)
        run(group)
        split(d, 0)

    forward(lot + 1)
    for copy in weights:
        copy.wait()
    hand_over(lot)
    crossing(lot)
    forward(lot + 2)
    join(lot)
    hand_over(lot + 1)
    att_y(0).start()
    for d in range(1, lot):
        hand_over(d)
    crossing(lot + 1)
    for d in range(lot):
        arrange(d, d * group)
    finish(lot)
    join(lot + 1)
    run(lot * group)
    forward(lot + 3)
    for d in range(1, lot):
        split(d, d * group)
        if d > 1:
            join(d - 1)
    split(0, 0)
    join(lot - 1)
    join(0)
    hand_over(lot + 2)
    finish(lot + 1)
    crossing(lot + 2)
    att_y(1).start()
    hand_over(lot + 3)
    join(lot + 2)
    crossing(lot + 3)
    finish(lot + 2)
    join(lot + 3)
    att_y(2).start()
    att_y(3).start()
    next_near = combiner(next_slot, next_share, 0, lot)
    for d in range(1, lot):
        rz_copy(d).wait_recv()
    for col in range(0, width, tile):
        near = retn[1 - hi, :, :, col : col + tile].reshape(lot * rows, tile)
        total = dot(next_near[0], near) + dot(next_near[1], near)
        nsend[:, col : col + tile] = total.astype(BF)
    for i in range(2):
        mix_y(i).start()
    finish(lot + 3)

    own_near = combiner(own_slot, own_share, 0, lot)
    own_far = combiner(own_slot, own_share, lot, ep)
    for d in range(lot, ep):
        rz_copy(d).wait_recv()
    for i in range(2):
        mix_y(i).wait_recv()
    for col in range(0, width, tile):
        near = retn[hi, :, :, col : col + tile].reshape(lot * rows, tile)
        far = retx[:, :, col : col + tile].reshape(lot * rows, tile)
        total = dot(own_near[0], near) + dot(own_near[1], near)
        total = total + dot(own_far[0], far) + dot(own_far[1], far)
        total = total + nrecv[:, col : col + tile].astype(F32)
        mixed[:, col : col + tile] = total.astype(BF)
    for i in range(pieces):
        att_y(i).wait_recv()
    whole = pbuf[core, hi].astype(F32) + abuf[hi].astype(F32) + arecv[...].astype(F32)
    attended[...] = whole.astype(BF)

    @pl.when(me < ep - 1)
    def _():
        k_halo.wait_send()
        v_halo.wait_send()

    for copy in [info_y, tok_y, att_d, mix_y(0), mix_y(1)] + [att_y(i) for i in range(pieces)]:
        copy.wait_send()
    for d in range(ep):
        rd_copy(d).wait_send()
        if d > 0:
            z_copy(d).wait_send()
            rz_copy(d).wait_send()
        if 0 < d < lot:
            n_copy(d).wait_send()
        if d >= lot:
            ry_copy(d).wait_send()


def run_fused(dims, tok, gain, info, sink, qgain, kgain, streams):
    ep, local, cap, rows, width, ffn, own, seq, kv_heads, q_heads, experts = dims
    lot = ep // 2
    order = np.arange(local * 4 * cap)
    e, t, c = order // (4 * cap), order // cap % 4, order % cap
    perm = (t * rows + e * cap + c)[:, None] == np.arange(4 * rows)[None, :]
    perm = jnp.asarray(perm, BF)
    dma = pltpu.SemaphoreType.DMA
    vm = pl.BlockSpec(memory_space=pltpu.VMEM)
    anys = pl.BlockSpec(memory_space=pl.ANY)
    kv_width = kv_heads * 64

    def held(*shape, dtype=BF):
        return pltpu.VMEM(shape, dtype)

    return pl.pallas_call(
        lambda *refs: fused_kernel(dims, *refs),
        name="fused_layer",
        out_shape=(
            jax.ShapeDtypeStruct((own, width), BF), jax.ShapeDtypeStruct((own, width), BF)
        ),
        in_specs=[vm, vm, vm, pl.BlockSpec(memory_space=pltpu.SMEM)] + [vm] * 4 + [anys] * 7,
        out_specs=(vm, vm),
        scratch_shapes=[
            held(local, width, ffn), held(local, width, ffn), held(local, ffn, width),
            held(q_heads * 64, width),
            held(seq, q_heads * 64),
            held(seq + WINDOW, kv_width), held(seq + WINDOW, kv_width),
            held(kv_heads, seq + WINDOW, 128), held(kv_heads, seq + WINDOW, 128),
            held(seq, q_heads * 64),
            held(ep, rows, width), held(lot, rows, width),
            held(own, width), held(8, own, dtype=F32), held(own, width),
            held(ep, 2, 2, rows, width),
            held(local, lot * 4 * cap, width),
            held(ep, 2, rows, width), held(ep, 2, rows, width),
            held(lot, rows, width),
            held(2, lot, rows, width), held(lot, rows, width),
            held(own, width), held(own, width),
            held(2, 2, own, width), held(2, own, width), held(own, width), held(own, width),
            dma((7,)),
            dma((ep,)), dma((ep,)),
            dma((lot,)), dma((lot,)),
            dma((lot,)), dma((lot,)),
            dma((ep,)), dma((ep,)),
            dma((ep,)), dma((ep,)),
            dma((lot,)), dma((lot,)),
            dma((ep,)), dma((ep,)),
            dma((12,)), dma((12,)),
        ],
        compiler_params=pltpu.CompilerParams(
            collective_id=0, has_side_effects=True, vmem_limit_bytes=67043328
        ),
    )(tok, gain, info, sink, qgain, kgain, perm, perm.T, *streams)


def fits(dims, tp, kv_size):
    ep, local, cap, rows, width, ffn, own, seq, kv_heads, q_heads, experts = dims
    if tp != 4 or ep < 4 or ep & (ep - 1) or rows % 16 or cap % 4 or kv_size != 64:
        return False
    if own != 128 or seq != 4 * own or kv_heads % 2 or q_heads != 3 * kv_heads or width % 512:
        return False
    lot = ep // 2
    held = 3 * local * width * ffn + q_heads * 64 * width + 3 * seq * q_heads * 64
    held += rows * width * (11 * ep + 5 * lot) + local * lot * 4 * cap * width + 14 * own * width
    return 2 * held < 63 * 1024 * 1024


def on_device(
    query_rows,
    key_rows,
    value_rows,
    query_gain,
    key_gain,
    sink_logits,
    out_weight,
    expert_input,
    expert_gain,
    routes,
    route_logits,
    gate_weight,
    up_weight,
    down_weight,
):
    own_rows = expert_input.shape[0]
    fanout = routes.shape[1]
    capacity = (3 * own_rows * fanout + 2 * EXPERTS - 1) // (2 * EXPERTS)
    ep_size = lax.axis_size("ep")
    tp_size = lax.axis_size("tp")
    local_experts = gate_weight.shape[0]
    key_heads, head_size = key_gain.shape
    dims = (
        ep_size, local_experts, capacity, local_experts * capacity, expert_input.shape[1],
        gate_weight.shape[2], own_rows, query_rows.shape[0], key_heads, query_gain.shape[0],
        EXPERTS,
    )
    if fits(dims, tp_size, head_size):
        info = jnp.concatenate(
            [routes.astype(F32), route_logits, jnp.zeros((own_rows, 4), F32)], axis=1
        ).T
        return run_fused(
            dims, expert_input, expert_gain.reshape(1, -1), info, sink_logits.reshape(1, -1),
            query_gain.reshape(-1, 2 * head_size), key_gain.reshape(-1, 2 * head_size),
            (query_rows, key_rows, value_rows, out_weight, gate_weight, up_weight, down_weight),
        )
    heads_out = attend(query_rows, key_rows, value_rows, query_gain, key_gain, sink_logits)
    projected = jnp.dot(heads_out, out_weight, preferred_element_type=jnp.float32).astype(
        jnp.bfloat16
    )
    widened = expert_input.astype(jnp.float32)
    normed = (
        widened
        * lax.rsqrt(jnp.mean(widened * widened, axis=-1, keepdims=True) + EPSILON)
        * expert_gain
    ).astype(jnp.bfloat16)
    route_weight = jax.nn.softmax(route_logits, axis=-1)
    attended = lax.psum_scatter(projected, "tp", scatter_dimension=0, tiled=True)
    combine = combine_matrix(routes, route_weight, capacity)
    sender = dispatch_matrix(routes, capacity)
    slot_rows = jnp.einsum(
        "ecr,rd->ecd", sender, normed, preferred_element_type=jnp.float32
    ).astype(jnp.bfloat16)
    slot_rows = slot_rows.reshape(ep_size, local_experts, capacity, -1)
    arrived = lax.all_to_all(slot_rows, "ep", split_axis=0, concat_axis=0, tiled=True)
    hidden_units = expert_hidden(
        lax.all_gather(arrived, "tp", axis=0, tiled=True), gate_weight, up_weight
    )
    partial_value = jnp.einsum(
        "aecf,efd->aecd", hidden_units, down_weight, preferred_element_type=jnp.float32
    ).astype(jnp.bfloat16)
    partial_value = partial_value.reshape(tp_size, ep_size * local_experts * capacity, -1)
    pieces = lax.all_to_all(partial_value, "tp", split_axis=0, concat_axis=0, tiled=True)
    summed = jnp.sum(pieces, axis=0, dtype=jnp.float32).astype(jnp.bfloat16)
    summed = summed.reshape(ep_size, local_experts * capacity, -1)
    returned = lax.all_to_all(summed, "ep", split_axis=0, concat_axis=0, tiled=True).reshape(
        EXPERTS, capacity, -1
    )
    expert_mix = jnp.einsum(
        "rec,ecd->rd", combine, returned.astype(jnp.float32), precision=lax.Precision.HIGHEST
    ).astype(jnp.bfloat16)
    return (attended, expert_mix)


def solution(mesh):
    placed = (
        P("ep", "tp"),
        P("ep", "tp"),
        P("ep", "tp"),
        P("tp", None),
        P("tp", None),
        P("tp"),
        P("tp", None),
        P(("ep", "tp"), None),
        P(),
        P(("ep", "tp"), None),
        P(("ep", "tp"), None),
        P("ep", None, "tp"),
        P("ep", None, "tp"),
        P("ep", "tp", None),
    )
    return jax.shard_map(
        on_device,
        mesh=mesh,
        in_specs=placed,
        out_specs=(P(("ep", "tp"), None), P(("ep", "tp"), None)),
        check_vma=False,
    )
```

time: 163 us -> 117 us (0.72)
  between operations: 14.5 us -> 0.65 us
  matrix products: 11.3 us -> 0 us
  Pallas kernels: 114 us -> 107 us
  other arithmetic: 8.93 us -> 2.02 us
  starting transfers between devices: 5.55 us -> 0 us
  local copies, waits for them, and re-layouts: 8.25 us -> 6.55 us
    dot_general x6 -> x0, matrix products: 11.3 us -> none  [the longest x1 3.26 us: on_device(): jnp.dot(combine, returned.astype(jnp.float32), precision=lax.Precision.HI...]
    pallas_call x1, Pallas kernels: 114 us -> 107 us  [run_fused(): pl.pallas_call(lambda *refs: fused_kernel(dims, *refs), name='fused_layer...]
    ppermute x1 -> x0, starting transfers between devices: 5.52 us -> none  [shifted(): lax.ppermute(value, axis, [(source, source + steps) for source in range(i...]
    reduce_sum x5 -> x0, other arithmetic: 3.51 us -> none  [the longest x2 1.69 us: head_norm(): jnp.mean(widened * widened, axis=-1, keepdims=True) + EPSILON]
    convert_element_type x5 -> x1, other arithmetic: 2.8 us -> 0.68 us  [on_device(): routes.astype(F32)]
    reshape x2, local copies, waits for them, and re-layouts: 0.66 us -> 2.71 us  [the longest x1 1.36 us: on_device(): query_gain.reshape(-1, 2 * head_size)]
    unnamed x34 -> x2, local copies, waits for them, and re-layouts: 3.4 us -> 3.76 us
  transfers between devices with their start and end apart: 2 -> 0, of which waited for: 0 -> 0; matrix products, arithmetic and copies ran while one was open for 9% -> 0% of each run, Pallas kernels for 70% -> 0%
where the time goes in v1:
time: 117 us; the launch traced here: 116 us
  Pallas kernels  107 us (91%)
  local copies, waits for them, and re-layouts  6.55 us (6%)
  other arithmetic  2.02 us (2%)
    pallas_call x1, Pallas kernels, run_fused(): pl.pallas_call(lambda *refs: fused_kernel(dims, *refs), name='fused_layer...  107 us
    unnamed x2, local copies, waits for them, and re-layouts  3.76 us

profile of v1, /device:TPU:0, one launch (start us, length us, event | category | flops | bytes accessed | tf_op | source)
XLA Modules:
  0.0 116.5 jit_solution(6439618797603102248)
XLA Ops:
  0.6 0.1 pad.2.clone
  0.7 1.4 %reshape.19.refs_5_ = f32[2,128]{1,0:T(2,128)} reshape(f32[4,64]{1,0:T(4,128)} %param.19) | data formatting | bytes 2048 | tf_op jit(solution)/shard_map/reshape | solution.py:673
  2.1 0.7 convert_element_type.3
  2.7 1.3 %maximum_bitcast_fusion.refs_2_ = f32[8,128]{1,0:T(8,128)} fusion(f32[128,2]{0,1:T(2,128)} %param.25, f32[128,2]{0,1:T(2,128)S(1)} %convert_element_type.3, f32[8]{0:T(128)S(1)} %pad.2.clone), kind=kLoop, calls=%fused_computation | loop fusion | flops 2048 | bytes 6176 | tf_op jit(solution)/shard_map/transpose | solution.py:670
  4.1 1.4 %reshape.18.refs_4_ = f32[6,128]{1,0:T(8,128)} reshape(f32[12,64]{1,0:T(8,128)} %param.18) | data formatting | bytes 6144 | tf_op jit(solution)/shard_map/reshape | solution.py:673
  5.4 107.2 %fused_layer.1 = (bf16[128,2048]{1,0:T(8,128)(2,1)}, bf16[128,2048]{1,0:T(8,128)(2,1)}) custom-call(bf16[128,2048]{1,0:T(8,128)(2,1)} %refs_0_.1, f32[1,2048]{1,0:T(1,128)} %bitcast.4, f32[8,128]{1,0:T(8,128)} %maximum_bitcast_fusion.refs_2_, f32[1,12]{1,0:T(1,128)} %bitcast.5, f32[6,128]{1,0:T(8,128)} %reshape.18.refs_4_, f32[2,128]{1,0:T(2,128)} %reshape.19.refs_5_, ...), custom_call_target="tpu_custom_call" | custom-call | tf_op jit(solution)/shard_map/fused_layer/pallas_call | solution.py:587
  112.7 1.9 %copy.19 = bf16[128,2048]{1,0:T(8,128)(2,1)} copy(bf16[128,2048]{1,0:T(8,128)(2,1)} %get-tuple-element.4) | data formatting | bytes 1048576
  114.6 1.9 %copy.20 = bf16[128,2048]{1,0:T(8,128)(2,1)} copy(bf16[128,2048]{1,0:T(8,128)(2,1)} %get-tuple-element.5) | data formatting | bytes 1048576
  (1 shorter events, 0.0 us)

commit v2 on v1

--- a/solution.py
+++ b/solution.py
@@ -111,6 +111,7 @@
     return (clipped * jax.nn.sigmoid(ACT_SLOPE * clipped) * (linear + 1.0)).astype(jnp.bfloat16)
 
 
+VMEM_LIMIT = 67043328
 MESH = pl.DeviceIdType.MESH
 BF = jnp.bfloat16
 F32 = jnp.float32
@@ -131,11 +132,11 @@
 
 
 def fused_kernel(
-    dims, tok, gain, info, sink, qgain, kgain, perm, unperm,
+    dims, tok, gain, routes, logits, sink, qgain, kgain, perm, unperm,
     q_hbm, k_hbm, v_hbm, wo_hbm, gate_hbm, up_hbm, down_hbm,
     attended, mixed,
-    gate_w, up_w, down_w, wo, qbuf, kext, vext, kd, vd, ho,
-    slots, nslots, ntok, ninfo, nrm, gath, xbuf, dbuf, sums, ybuf, retn, retx,
+    qpair, gate_w, up_w, down_w, wo, qbuf, kext, vext, kd, vd, ho,
+    slots, nslots, ntok, nroutes, nlogits, nrm, gath, xbuf, dbuf, sums, ybuf, retn, retx,
     nsend, nrecv, pbuf, abuf, asend, arecv,
     lsem, zs, zr, ns, nr, ys, yr, ds, dr, rds, rdr, rys, ryr, rzs, rzr, ms, mr,
 ):
@@ -153,12 +154,16 @@
     across = (me, (1 - hi) * 2 + core)
 
     def mate(d):
-        found, bit = me, 1
+        found, bit = 0, 1
         while bit < ep:
-            if d & bit:
-                found = found + bit - 2 * bit * (me // bit % 2)
+            found = found + (me // bit + d // bit) % 2 * bit
             bit *= 2
         return found
+
+    inner = (me // (ep // 4) + 1) // 2 % 2
+
+    def far(i):
+        return lot + (i + lot // 2) % lot
 
     def remote(src, dst, send, recv, device):
         return pltpu.make_async_remote_copy(
@@ -177,7 +182,8 @@
         pltpu.make_async_copy(down_hbm, down_w, lsem.at[6]),
     ]
 
-    info_y = remote(info, ninfo, ms.at[0], mr.at[0], across)
+    routes_y = remote(routes, nroutes, ms.at[0], mr.at[0], across)
+    logits_y = remote(logits, nlogits, ms.at[5], mr.at[5], across)
     tok_y = remote(tok, ntok, ms.at[1], mr.at[1], across)
     following = ((me + 1) % ep, tp)
     k_halo = remote(
@@ -220,12 +226,14 @@
             sums.at[d, 1 - hi], ybuf.at[d - lot], rys.at[d - lot], ryr.at[d - lot], across
         )
 
+    def near_copy(d):
+        return remote(sums.at[d], retn.at[:, d], rzs.at[d], rzr.at[d], (mate(d), tp))
+
     def rz_copy(d):
-        if d < lot:
-            return remote(sums.at[d], retn.at[:, d], rzs.at[d], rzr.at[d], (mate(d), tp))
         return remote(sums.at[d, hi], retx.at[d - lot], rzs.at[d], rzr.at[d], (mate(d), tp))
 
-    def placed(table):
+    def placed(routed, scores):
+        table = routed.astype(F32)
         expert_ids = iota((experts, own), 0).astype(F32)
         hot = [(table[k : k + 1] == expert_ids).astype(F32) for k in range(2)]
         earlier = (iota((own, own), 0) < iota((own, own), 1)).astype(BF)
@@ -234,8 +242,8 @@
             table[k : k + 1] * cap + jnp.sum(before * hot[k], axis=0, keepdims=True)
             for k in range(2)
         ]
-        top = jnp.maximum(table[2:3], table[3:4])
-        raised = [jnp.exp(table[2 + k : 3 + k] - top) for k in range(2)]
+        top = jnp.maximum(scores[0:1], scores[1:2])
+        raised = [jnp.exp(scores[k : k + 1] - top) for k in range(2)]
         share = [raised[k] / (raised[0] + raised[1]) for k in range(2)]
         return slot, share
 
@@ -277,7 +285,7 @@
     pl.semaphore_signal(barrier, inc=1, device_id=across, device_id_type=MESH)
     pl.semaphore_signal(barrier, inc=1, device_id=partner, device_id_type=MESH)
 
-    own_slot, own_share = placed(info[...])
+    own_slot, own_share = placed(routes[...], logits[...])
     normalise(tok)
     own_pick = picker(own_slot, 0, ep)
     for col in range(0, width, tile):
@@ -286,7 +294,8 @@
         gath[0, core, hi, :, col : col + tile] = picked[:rows]
 
     pl.semaphore_wait(barrier, ep + 1)
-    info_y.start()
+    routes_y.start()
+    logits_y.start()
     tok_y.start()
 
     @pl.when(me < ep - 1)
@@ -294,13 +303,21 @@
         k_halo.start()
         v_halo.start()
 
-    for d in list(range(lot, ep)) + list(range(1, lot)):
+    for i in range(lot // 2):
+        z_copy(far(i)).start()
+    for d in range(1, lot):
         z_copy(d).start()
     for copy in weights:
         copy.start()
 
     low_half = iota((1, 128), 1) < 64
     same_head = (iota((128, 128), 0) // 64 == iota((128, 128), 1) // 64).astype(BF)
+
+    def gain_pair(table, t):
+        return jnp.concatenate([table[2 * t : 2 * t + 1], table[2 * t + 1 : 2 * t + 2]], axis=1)
+
+    for t in range(pairs):
+        qpair[t : t + 1] = gain_pair(qgain, t)
 
     def head_scaled(block, gain_row):
         wide = block.astype(F32)
@@ -318,7 +335,7 @@
     def prepare(start, count):
         for m in range(kv_heads // 2):
             cols = slice(m * 128, (m + 1) * 128)
-            keys = head_scaled(kext[pl.ds(start, count), cols], kgain[m : m + 1])
+            keys = head_scaled(kext[pl.ds(start, count), cols], gain_pair(kgain, m))
             spread(keys.astype(BF).astype(F32), kd, m, start, count)
             spread(vext[pl.ds(start, count), cols].astype(F32), vd, m, start, count)
 
@@ -334,7 +351,7 @@
         for j in range(tiles):
             lane = pl.multiple_of((m * tiles + j) * 128, 128)
             scaled = head_scaled(
-                qbuf[pl.ds(top_row, WINDOW), pl.ds(lane, 128)], qgain[pl.ds(m * tiles + j, 1)]
+                qbuf[pl.ds(top_row, WINDOW), pl.ds(lane, 128)], qpair[pl.ds(m * tiles + j, 1)]
             ).astype(BF).astype(F32) * 0.125
             outs = []
             for half in range(2):
@@ -382,14 +399,20 @@
             prepare(0, halo)
 
         lax.fori_loop(0, kv_heads // 2, lambda m, c: (attend_pair(b, m), c)[1], 0)
+
         return carry
 
     def forward(d):
         z_copy(d).wait_recv()
         y_copy(d).start()
 
+    def at_edge(step):
+        pl.when(inner == 0)(step)
+
+    def at_middle(step):
+        pl.when(inner == 1)(step)
+
     lax.fori_loop(0, blocks, attend_block, 0)
-    forward(lot)
     wo_in.wait()
 
     def project(i, carry):
@@ -402,9 +425,11 @@
     lax.fori_loop(0, width // 256, project, 0)
     att_d.start()
 
-    info_y.wait_recv()
+    forward(far(0))
+    routes_y.wait_recv()
+    logits_y.wait_recv()
     tok_y.wait_recv()
-    next_slot, next_share = placed(ninfo[...])
+    next_slot, next_share = placed(nroutes[...], nlogits[...])
     normalise(ntok)
     next_pick = picker(next_slot, 0, lot)
     for col in range(0, width, tile):
@@ -413,11 +438,13 @@
         gath[0, core, 1 - hi, :, col : col + tile] = picked[:rows]
     for d in range(1, lot):
         n_copy(d).start()
+    for i in range(lot // 2, lot):
+        z_copy(far(i)).start()
     d_copy(0).start()
 
+    forward(far(1))
     att_d.wait_recv()
     asend[...] = (pbuf[core, 1 - hi].astype(F32) + abuf[1 - hi].astype(F32)).astype(BF)
-
     def arrange(d, at):
         d_copy(d).wait_recv()
         for col in range(0, width, tile):
@@ -426,21 +453,21 @@
             for e in range(local):
                 xbuf[e, at : at + group, col : col + tile] = moved[e * group : (e + 1) * group]
 
-    def run(count):
+    def run(at, count, first=0, last=local):
         def expert(e, carry):
-            x = xbuf[e, 0:count]
+            x = xbuf[e, at : at + count]
             hidden = activation(dot(x, gate_w[e]), dot(x, up_w[e]))
             for col in range(0, width, tile):
-                xbuf[e, 0:count, col : col + tile] = dot(
+                xbuf[e, at : at + count, col : col + tile] = dot(
                     hidden, down_w[e, :, col : col + tile]
                 ).astype(BF)
             return carry
 
-        lax.fori_loop(0, local, expert, 0)
-
-    def split(d, at):
+        lax.fori_loop(first, last, expert, 0)
+
+    def split(d, at, crossed):
         d_copy(d).wait_send()
-        if d >= lot:
+        if crossed:
             y_copy(d).wait_send()
         for col in range(0, width, tile):
             block = jnp.concatenate(
@@ -452,11 +479,12 @@
 
     def join(d):
         rd_copy(d).wait_recv()
-        if d >= lot:
-            part = gath[d, core, 1 - hi].astype(F32) + dbuf[d, 1 - hi].astype(F32)
-            sums[d, 1 - hi] = part.astype(BF)
-            ry_copy(d).start()
-            return
+        part = gath[d, core, 1 - hi].astype(F32) + dbuf[d, 1 - hi].astype(F32)
+        sums[d, 1 - hi] = part.astype(BF)
+        ry_copy(d).start()
+
+    def near_join(d):
+        rd_copy(d).wait_recv()
         for h in range(2):
             part = (gath[d, core, h].astype(F32) + dbuf[d, h].astype(F32)).astype(BF)
             if d == 0:
@@ -464,7 +492,7 @@
             else:
                 sums[d, h] = part
         if d > 0:
-            rz_copy(d).start()
+            near_copy(d).start()
 
     def finish(d):
         ry_copy(d).wait_recv()
@@ -473,65 +501,74 @@
         rz_copy(d).start()
 
     def hand_over(d):
-        if d >= lot:
-            y_copy(d).wait_recv()
-        elif d > 0:
-            z_copy(d).wait_recv()
-            n_copy(d).wait_recv()
-        if d > 0:
-            d_copy(d).start()
-
-    def crossing(d):
-        arrange(d, 0)
-        run(group)
-        split(d, 0)
-
-    forward(lot + 1)
+        y_copy(d).wait_recv()
+        d_copy(d).start()
+
+    def near_hand_over(d):
+        z_copy(d).wait_recv()
+        n_copy(d).wait_recv()
+        d_copy(d).start()
+
+    def near_sum():
+        near_pick = combiner(next_slot, next_share, 0, lot)
+        for d in range(1, lot):
+            near_copy(d).wait_recv()
+        for col in range(0, width, tile):
+            near = retn[1 - hi, :, :, col : col + tile].reshape(lot * rows, tile)
+            total = dot(near_pick[0], near) + dot(near_pick[1], near)
+            nsend[:, col : col + tile] = total.astype(BF)
+        for i in range(2):
+            mix_y(i).start()
+
+    att_y(0).start()
+    att_y(1).start()
     for copy in weights:
         copy.wait()
-    hand_over(lot)
-    crossing(lot)
-    forward(lot + 2)
-    join(lot)
-    hand_over(lot + 1)
-    att_y(0).start()
+    hand_over(far(0))
+    arrange(far(0), 0)
+    run(0, group)
+    hand_over(far(1))
+    split(far(0), 0, True)
+    arrange(far(1), 0)
+    join(far(0))
+    run(0, group)
     for d in range(1, lot):
-        hand_over(d)
-    crossing(lot + 1)
-    for d in range(lot):
+        near_hand_over(d)
+    split(far(1), 0, True)
+    forward(far(2))
+    arrange(0, 0)
+    join(far(1))
+    finish(far(0))
+    for d in range(1, lot):
         arrange(d, d * group)
-    finish(lot)
-    join(lot + 1)
-    run(lot * group)
-    forward(lot + 3)
-    for d in range(1, lot):
-        split(d, d * group)
-        if d > 1:
-            join(d - 1)
-    split(0, 0)
-    join(lot - 1)
-    join(0)
-    hand_over(lot + 2)
-    finish(lot + 1)
-    crossing(lot + 2)
-    att_y(1).start()
-    hand_over(lot + 3)
-    join(lot + 2)
-    crossing(lot + 3)
-    finish(lot + 2)
-    join(lot + 3)
+    run(0, lot * group, 0, 2)
+    forward(far(3))
     att_y(2).start()
     att_y(3).start()
-    next_near = combiner(next_slot, next_share, 0, lot)
-    for d in range(1, lot):
-        rz_copy(d).wait_recv()
-    for col in range(0, width, tile):
-        near = retn[1 - hi, :, :, col : col + tile].reshape(lot * rows, tile)
-        total = dot(next_near[0], near) + dot(next_near[1], near)
-        nsend[:, col : col + tile] = total.astype(BF)
-    for i in range(2):
-        mix_y(i).start()
-    finish(lot + 3)
+    run(0, lot * group, 2, 4)
+    split(1, group, False)
+    split(2, 2 * group, False)
+    hand_over(far(2))
+    near_join(1)
+    split(3, 3 * group, False)
+    near_join(2)
+    split(0, 0, False)
+    arrange(far(2), 0)
+    near_join(3)
+    finish(far(1))
+    run(0, group)
+    split(far(2), 0, True)
+    hand_over(far(3))
+    arrange(far(3), group)
+    join(far(2))
+    run(group, group, 0, 3)
+    near_join(0)
+    finish(far(2))
+    run(group, group, 3, 4)
+    split(far(3), group, True)
+    join(far(3))
+    finish(far(3))
+    near_sum()
 
     own_near = combiner(own_slot, own_share, 0, lot)
     own_far = combiner(own_slot, own_share, lot, ep)
@@ -556,20 +593,21 @@
         k_halo.wait_send()
         v_halo.wait_send()
 
-    for copy in [info_y, tok_y, att_d, mix_y(0), mix_y(1)] + [att_y(i) for i in range(pieces)]:
+    for copy in [routes_y, logits_y, tok_y, att_d, mix_y(0), mix_y(1)] + [att_y(i) for i in range(pieces)]:
         copy.wait_send()
     for d in range(ep):
         rd_copy(d).wait_send()
         if d > 0:
             z_copy(d).wait_send()
-            rz_copy(d).wait_send()
         if 0 < d < lot:
             n_copy(d).wait_send()
+            near_copy(d).wait_send()
         if d >= lot:
             ry_copy(d).wait_send()
-
-
-def run_fused(dims, tok, gain, info, sink, qgain, kgain, streams):
+            rz_copy(d).wait_send()
+
+
+def run_fused(dims, tok, gain, routes, logits, sink, qgain, kgain, streams):
     ep, local, cap, rows, width, ffn, own, seq, kv_heads, q_heads, experts = dims
     lot = ep // 2
     order = np.arange(local * 4 * cap)
@@ -590,9 +628,10 @@
         out_shape=(
             jax.ShapeDtypeStruct((own, width), BF), jax.ShapeDtypeStruct((own, width), BF)
         ),
-        in_specs=[vm, vm, vm, pl.BlockSpec(memory_space=pltpu.SMEM)] + [vm] * 4 + [anys] * 7,
+        in_specs=[vm, vm, vm, vm, pl.BlockSpec(memory_space=pltpu.SMEM)] + [vm] * 4 + [anys] * 7,
         out_specs=(vm, vm),
         scratch_shapes=[
+            held(q_heads // 2, 128, dtype=F32),
             held(local, width, ffn), held(local, width, ffn), held(local, ffn, width),
             held(q_heads * 64, width),
             held(seq, q_heads * 64),
@@ -600,7 +639,7 @@
             held(kv_heads, seq + WINDOW, 128), held(kv_heads, seq + WINDOW, 128),
             held(seq, q_heads * 64),
             held(ep, rows, width), held(lot, rows, width),
-            held(own, width), held(8, own, dtype=F32), held(own, width),
+            held(own, width), held(2, own, dtype=jnp.int32), held(2, own, dtype=F32), held(own, width),
             held(ep, 2, 2, rows, width),
             held(local, lot * 4 * cap, width),
             held(ep, 2, rows, width), held(ep, 2, rows, width),
@@ -619,9 +658,9 @@
             dma((12,)), dma((12,)),
         ],
         compiler_params=pltpu.CompilerParams(
-            collective_id=0, has_side_effects=True, vmem_limit_bytes=67043328
+            collective_id=0, has_side_effects=True, vmem_limit_bytes=VMEM_LIMIT
         ),
-    )(tok, gain, info, sink, qgain, kgain, perm, perm.T, *streams)
+    )(tok, gain, routes, logits, sink, qgain, kgain, perm, perm.T, *streams)
 
 
 def fits(dims, tp, kv_size):
@@ -665,12 +704,9 @@
         EXPERTS,
     )
     if fits(dims, tp_size, head_size):
-        info = jnp.concatenate(
-            [routes.astype(F32), route_logits, jnp.zeros((own_rows, 4), F32)], axis=1
-        ).T
         return run_fused(
-            dims, expert_input, expert_gain.reshape(1, -1), info, sink_logits.reshape(1, -1),
-            query_gain.reshape(-1, 2 * head_size), key_gain.reshape(-1, 2 * head_size),
+            dims, expert_input, expert_gain.reshape(1, -1), routes.T, route_logits.T,
+            sink_logits.reshape(1, -1), query_gain, key_gain,
             (query_rows, key_rows, value_rows, out_weight, gate_weight, up_weight, down_weight),
         )
     heads_out = attend(query_rows, key_rows, value_rows, query_gain, key_gain, sink_logits)

time: 117 us -> 102 us (0.87)
  Pallas kernels: 107 us -> 97.5 us
  local copies, waits for them, and re-layouts: 6.55 us -> 3.76 us
  other arithmetic: 2.02 us -> 0 us
    pallas_call x1, Pallas kernels: 107 us -> 97.5 us  [run_fused(): pl.pallas_call(lambda *refs: fused_kernel(dims, *refs), name='fused_layer...]
    reshape x2 -> x0, local copies, waits for them, and re-layouts: 2.71 us -> none  [the longest x1 1.36 us: on_device(): query_gain.reshape(-1, 2 * head_size)]
    transpose x1 -> x0, other arithmetic: 1.34 us -> none  [on_device(): info = jnp.concatenate([routes.astype(F32), route_logits, jnp.zeros((own_...]
where the time goes in v2:
time: 102 us
  Pallas kernels  97.5 us (96%)
  local copies, waits for them, and re-layouts  3.76 us (4%)
    pallas_call x1, Pallas kernels, run_fused(): pl.pallas_call(lambda *refs: fused_kernel(dims, *refs), name='fused_layer...  97.5 us
    unnamed x2, local copies, waits for them, and re-layouts  3.76 us

profile of v2, /device:TPU:0, one launch (start us, length us, event | category | flops | bytes accessed | tf_op | source)
XLA Modules:
  0.0 101.9 jit_solution(5053636274023302474)
XLA Ops:
  0.6 97.5 %fused_layer.1 = (bf16[128,2048]{1,0:T(8,128)(2,1)}, bf16[128,2048]{1,0:T(8,128)(2,1)}) custom-call(bf16[128,2048]{1,0:T(8,128)(2,1)} %refs_0_.1, f32[1,2048]{1,0:T(1,128)} %bitcast.4, s32[2,128]{1,0:T(2,128)} %bitcast.5, f32[2,128]{1,0:T(2,128)} %bitcast.6, f32[1,12]{1,0:T(1,128)} %bitcast.7, f32[12,64]{1,0:T(8,128)} %refs_5_.1, f32[4,64]{1,0:T(4,128)} %refs_6_.1, ...), custom_call_target="tpu_custom_call" | custom-call | tf_op jit(solution)/shard_map/fused_layer/pallas_call | solution.py:625
  98.1 1.9 %copy.19 = bf16[128,2048]{1,0:T(8,128)(2,1)} copy(bf16[128,2048]{1,0:T(8,128)(2,1)} %get-tuple-element.4) | data formatting | bytes 1048576
  100.0 1.9 %copy.20 = bf16[128,2048]{1,0:T(8,128)(2,1)} copy(bf16[128,2048]{1,0:T(8,128)(2,1)} %get-tuple-element.5) | data formatting | bytes 1048576

commit v3 on v2

--- a/solution.py
+++ b/solution.py
@@ -137,7 +137,7 @@
     attended, mixed,
     qpair, gate_w, up_w, down_w, wo, qbuf, kext, vext, kd, vd, ho,
     slots, nslots, ntok, nroutes, nlogits, nrm, gath, xbuf, dbuf, sums, ybuf, retn, retx,
-    nsend, nrecv, pbuf, abuf, asend, arecv,
+    nsend, nrecv, pbuf, abuf, asend, arecv, partial,
     lsem, zs, zr, ns, nr, ys, yr, ds, dr, rds, rdr, rys, ryr, rzs, rzr, ms, mr,
 ):
     ep, local, cap, rows, width, ffn, own, seq, kv_heads, q_heads, experts = dims
@@ -303,8 +303,7 @@
         k_halo.start()
         v_halo.start()
 
-    for i in range(lot // 2):
-        z_copy(far(i)).start()
+    z_copy(far(0)).start()
     for d in range(1, lot):
         z_copy(d).start()
     for copy in weights:
@@ -438,11 +437,10 @@
         gath[0, core, 1 - hi, :, col : col + tile] = picked[:rows]
     for d in range(1, lot):
         n_copy(d).start()
-    for i in range(lot // 2, lot):
+    for i in range(1, lot):
         z_copy(far(i)).start()
     d_copy(0).start()
 
-    forward(far(1))
     att_d.wait_recv()
     asend[...] = (pbuf[core, 1 - hi].astype(F32) + abuf[1 - hi].astype(F32)).astype(BF)
     def arrange(d, at):
@@ -527,66 +525,73 @@
     hand_over(far(0))
     arrange(far(0), 0)
     run(0, group)
-    hand_over(far(1))
     split(far(0), 0, True)
-    arrange(far(1), 0)
-    join(far(0))
-    run(0, group)
     for d in range(1, lot):
         near_hand_over(d)
-    split(far(1), 0, True)
-    forward(far(2))
     arrange(0, 0)
-    join(far(1))
-    finish(far(0))
+    join(far(0))
+    forward(far(1))
     for d in range(1, lot):
         arrange(d, d * group)
     run(0, lot * group, 0, 2)
+    run(0, lot * group, 2, 3)
+    forward(far(2))
+    finish(far(0))
+    run(0, lot * group, 3, 4)
+    for d in range(1, lot):
+        split(d, d * group, False)
+    hand_over(far(1))
+    split(0, 0, False)
     forward(far(3))
+    for d in range(1, lot):
+        near_join(d)
     att_y(2).start()
     att_y(3).start()
-    run(0, lot * group, 2, 4)
-    split(1, group, False)
-    split(2, 2 * group, False)
+    arrange(far(1), 0)
     hand_over(far(2))
-    near_join(1)
-    split(3, 3 * group, False)
-    near_join(2)
-    split(0, 0, False)
-    arrange(far(2), 0)
-    near_join(3)
+    near_join(0)
+    arrange(far(2), group)
+    run(0, 2 * group)
+    hand_over(far(3))
+    split(far(1), 0, True)
+    split(far(2), group, True)
+    arrange(far(3), 0)
+    join(far(1))
+    join(far(2))
+    run(0, group, 0, 2)
     finish(far(1))
-    run(0, group)
-    split(far(2), 0, True)
-    hand_over(far(3))
-    arrange(far(3), group)
-    join(far(2))
-    run(group, group, 0, 3)
-    near_join(0)
+    run(0, group, 2, 4)
+    split(far(3), 0, True)
     finish(far(2))
-    run(group, group, 3, 4)
-    split(far(3), group, True)
     join(far(3))
+    near_sum()
     finish(far(3))
-    near_sum()
-
+
+    half = lot // 2
     own_near = combiner(own_slot, own_share, 0, lot)
-    own_far = combiner(own_slot, own_share, lot, ep)
-    for d in range(lot, ep):
-        rz_copy(d).wait_recv()
-    for i in range(2):
-        mix_y(i).wait_recv()
+    own_late = combiner(own_slot, own_share, lot, lot + half)
+    own_early = combiner(own_slot, own_share, lot + half, ep)
+    for i in range(half):
+        rz_copy(far(i)).wait_recv()
     for col in range(0, width, tile):
         near = retn[hi, :, :, col : col + tile].reshape(lot * rows, tile)
-        far = retx[:, :, col : col + tile].reshape(lot * rows, tile)
+        early = retx[half:, :, col : col + tile].reshape(half * rows, tile)
         total = dot(own_near[0], near) + dot(own_near[1], near)
-        total = total + dot(own_far[0], far) + dot(own_far[1], far)
-        total = total + nrecv[:, col : col + tile].astype(F32)
-        mixed[:, col : col + tile] = total.astype(BF)
+        total = total + dot(own_early[0], early) + dot(own_early[1], early)
+        partial[:, col : col + tile] = total
     for i in range(pieces):
         att_y(i).wait_recv()
     whole = pbuf[core, hi].astype(F32) + abuf[hi].astype(F32) + arecv[...].astype(F32)
     attended[...] = whole.astype(BF)
+    for i in range(half, lot):
+        rz_copy(far(i)).wait_recv()
+    for i in range(2):
+        mix_y(i).wait_recv()
+    for col in range(0, width, tile):
+        late = retx[:half, :, col : col + tile].reshape(half * rows, tile)
+        total = partial[:, col : col + tile] + nrecv[:, col : col + tile].astype(F32)
+        total = total + dot(own_late[0], late) + dot(own_late[1], late)
+        mixed[:, col : col + tile] = total.astype(BF)
 
     @pl.when(me < ep - 1)
     def _():
@@ -647,6 +652,7 @@
             held(2, lot, rows, width), held(lot, rows, width),
             held(own, width), held(own, width),
             held(2, 2, own, width), held(2, own, width), held(own, width), held(own, width),
+            held(own, width, dtype=F32),
             dma((7,)),
             dma((ep,)), dma((ep,)),
             dma((lot,)), dma((lot,)),
@@ -663,6 +669,47 @@
     )(tok, gain, routes, logits, sink, qgain, kgain, perm, perm.T, *streams)
 
 
+def hand_out(first, second):
+    count = 2
+    rows, width = first.shape
+    piece = rows // count
+
+    def kernel(first_in, second_in, first_out, second_out, held, sem_in, sem_out):
+        pairs = ((first_in, first_out), (second_in, second_out))
+        steps = [(a, i) for a in range(2) for i in range(count)]
+
+        def inward(a, i):
+            at = pl.ds(i * piece, piece)
+            return pltpu.make_async_copy(pairs[a][0].at[at], held.at[a, at], sem_in.at[a, i])
+
+        def outward(a, i):
+            at = pl.ds(i * piece, piece)
+            return pltpu.make_async_copy(held.at[a, at], pairs[a][1].at[at], sem_out.at[a, i])
+
+        for step in steps:
+            inward(*step).start()
+        for step in steps:
+            inward(*step).wait()
+            outward(*step).start()
+        for step in steps:
+            outward(*step).wait()
+
+    anys = pl.BlockSpec(memory_space=pl.ANY)
+    shape = jax.ShapeDtypeStruct(first.shape, first.dtype)
+    return pl.pallas_call(
+        kernel,
+        name="hand_out",
+        out_shape=(shape, shape),
+        in_specs=[anys, anys],
+        out_specs=(anys, anys),
+        scratch_shapes=[
+            pltpu.VMEM((2, rows, width), BF),
+            pltpu.SemaphoreType.DMA((2, count)),
+            pltpu.SemaphoreType.DMA((2, count)),
+        ],
+    )(first, second)
+
+
 def fits(dims, tp, kv_size):
     ep, local, cap, rows, width, ffn, own, seq, kv_heads, q_heads, experts = dims
     if tp != 4 or ep < 4 or ep & (ep - 1) or rows % 16 or cap % 4 or kv_size != 64:
@@ -671,7 +718,7 @@
         return False
     lot = ep // 2
     held = 3 * local * width * ffn + q_heads * 64 * width + 3 * seq * q_heads * 64
-    held += rows * width * (11 * ep + 5 * lot) + local * lot * 4 * cap * width + 14 * own * width
+    held += rows * width * (11 * ep + 5 * lot) + local * lot * 4 * cap * width + 16 * own * width
     return 2 * held < 63 * 1024 * 1024
 
 
@@ -704,11 +751,12 @@
         EXPERTS,
     )
     if fits(dims, tp_size, head_size):
-        return run_fused(
+        results = run_fused(
             dims, expert_input, expert_gain.reshape(1, -1), routes.T, route_logits.T,
             sink_logits.reshape(1, -1), query_gain, key_gain,
             (query_rows, key_rows, value_rows, out_weight, gate_weight, up_weight, down_weight),
         )
+        return hand_out(*results)
     heads_out = attend(query_rows, key_rows, value_rows, query_gain, key_gain, sink_logits)
     projected = jnp.dot(heads_out, out_weight, preferred_element_type=jnp.float32).astype(
         jnp.bfloat16

time: 102 us -> 99.4 us (0.975)
  local copies, waits for them, and re-layouts: 3.76 us -> 0 us
    unnamed x2 -> x0, local copies, waits for them, and re-layouts: 3.76 us -> none
    pallas_call x0 -> x1, Pallas kernels: none -> 1.98 us  [hand_out(): pl.pallas_call(kernel, name='hand_out', out_shape=(shape, shape), in_spec...]
    pallas_call x1, Pallas kernels: 97.5 us -> 96.3 us  [run_fused(): pl.pallas_call(lambda *refs: fused_kernel(dims, *refs), name='fused_layer...]
where the time goes in v3:
time: 99.4 us; the launch traced here: 99.1 us
  Pallas kernels  98.3 us (99%)
    pallas_call x1, Pallas kernels, run_fused(): pl.pallas_call(lambda *refs: fused_kernel(dims, *refs), name='fused_layer...  96.3 us

profile of v3, /device:TPU:0, one launch (start us, length us, event | category | flops | bytes accessed | tf_op | source)
XLA Modules:
  0.0 99.1 jit_solution(17493663479803686973)
XLA Ops:
  0.6 96.3 %fused_layer.1 = (bf16[128,2048]{1,0:T(8,128)(2,1)}, bf16[128,2048]{1,0:T(8,128)(2,1)}) custom-call(bf16[128,2048]{1,0:T(8,128)(2,1)} %refs_0_.1, f32[1,2048]{1,0:T(1,128)} %bitcast.4, s32[2,128]{1,0:T(2,128)} %bitcast.5, f32[2,128]{1,0:T(2,128)} %bitcast.6, f32[1,12]{1,0:T(1,128)} %bitcast.7, f32[12,64]{1,0:T(8,128)} %refs_5_.1, f32[4,64]{1,0:T(4,128)} %refs_6_.1, ...), custom_call_target="tpu_custom_call" | custom-call | tf_op jit(solution)/shard_map/fused_layer/pallas_call | solution.py:630
  97.0 2.0 %hand_out.1 = (bf16[128,2048]{1,0:T(8,128)(2,1)}, bf16[128,2048]{1,0:T(8,128)(2,1)}) custom-call(bf16[128,2048]{1,0:T(8,128)(2,1)} %get-tuple-element.4.first_in, bf16[128,2048]{1,0:T(8,128)(2,1)} %get-tuple-element.5.second_in), custom_call_target="tpu_custom_call" | custom-call | tf_op jit(solution)/shard_map/hand_out/pallas_call | solution.py:699

commit v4 on v3

--- a/solution.py
+++ b/solution.py
@@ -132,9 +132,10 @@
 
 
 def fused_kernel(
-    dims, tok, gain, routes, logits, sink, qgain, kgain, perm, unperm,
+    dims, tok_in, gain_in, routes_in, logits_in, sink_in, qgain_in, kgain_in, perm_in, unperm_in,
     q_hbm, k_hbm, v_hbm, wo_hbm, gate_hbm, up_hbm, down_hbm,
     attended, mixed,
+    tok, gain, routes, logits, sink, qgain, kgain, perm, unperm,
     qpair, gate_w, up_w, down_w, wo, qbuf, kext, vext, kd, vd, ho,
     slots, nslots, ntok, nroutes, nlogits, nrm, gath, xbuf, dbuf, sums, ybuf, retn, retx,
     nsend, nrecv, pbuf, abuf, asend, arecv, partial,
@@ -277,7 +278,15 @@
         mean = jnp.mean(wide * wide, axis=-1, keepdims=True)
         nrm[...] = (wide * lax.rsqrt(mean + EPSILON) * gain[...]).astype(BF)
 
-    for copy in (k_in, v_in, q_in, wo_in):
+    sources = (
+        tok_in, routes_in, logits_in, gain_in, sink_in, qgain_in, kgain_in, perm_in, unperm_in
+    )
+    targets = (tok, routes, logits, gain, sink, qgain, kgain, perm, unperm)
+    small = [
+        pltpu.make_async_copy(source, target, lsem.at[7 + i])
+        for i, (source, target) in enumerate(zip(sources, targets))
+    ]
+    for copy in small:
         copy.start()
     barrier = pltpu.get_barrier_semaphore()
     for d in range(1, ep):
@@ -285,6 +294,10 @@
     pl.semaphore_signal(barrier, inc=1, device_id=across, device_id_type=MESH)
     pl.semaphore_signal(barrier, inc=1, device_id=partner, device_id_type=MESH)
 
+    for copy in (k_in, v_in, q_in, wo_in):
+        copy.start()
+    for copy in small:
+        copy.wait()
     own_slot, own_share = placed(routes[...], logits[...])
     normalise(tok)
     own_pick = picker(own_slot, 0, ep)
@@ -518,6 +531,7 @@
         for i in range(2):
             mix_y(i).start()
 
+    near_order = list(range(2, lot)) + [1]
     att_y(0).start()
     att_y(1).start()
     for copy in weights:
@@ -538,12 +552,12 @@
     forward(far(2))
     finish(far(0))
     run(0, lot * group, 3, 4)
-    for d in range(1, lot):
+    for d in near_order:
         split(d, d * group, False)
     hand_over(far(1))
     split(0, 0, False)
     forward(far(3))
-    for d in range(1, lot):
+    for d in near_order:
         near_join(d)
     att_y(2).start()
     att_y(3).start()
@@ -633,9 +647,14 @@
         out_shape=(
             jax.ShapeDtypeStruct((own, width), BF), jax.ShapeDtypeStruct((own, width), BF)
         ),
-        in_specs=[vm, vm, vm, vm, pl.BlockSpec(memory_space=pltpu.SMEM)] + [vm] * 4 + [anys] * 7,
+        in_specs=[anys] * 16,
         out_specs=(vm, vm),
         scratch_shapes=[
+            held(own, width), held(1, width, dtype=F32),
+            held(2, own, dtype=jnp.int32), held(2, own, dtype=F32),
+            pltpu.SMEM((1, q_heads), F32),
+            held(q_heads, 64, dtype=F32), held(kv_heads, 64, dtype=F32),
+            held(4 * rows, 4 * rows), held(4 * rows, 4 * rows),
             held(q_heads // 2, 128, dtype=F32),
             held(local, width, ffn), held(local, width, ffn), held(local, ffn, width),
             held(q_heads * 64, width),
@@ -653,7 +672,7 @@
             held(own, width), held(own, width),
             held(2, 2, own, width), held(2, own, width), held(own, width), held(own, width),
             held(own, width, dtype=F32),
-            dma((7,)),
+            dma((16,)),
             dma((ep,)), dma((ep,)),
             dma((lot,)), dma((lot,)),
             dma((lot,)), dma((lot,)),

time: 99.4 us -> 99.1 us (level); the launches traced: 99.1 us -> 97.8 us
  Pallas kernels: 98.3 us -> 97 us
    pallas_call x1, Pallas kernels: 96.3 us -> 95 us  [run_fused(): pl.pallas_call(lambda *refs: fused_kernel(dims, *refs), name='fused_layer...]
where the time goes in v4:
time: 99.1 us; the launch traced here: 97.8 us
  Pallas kernels  97 us (98%)
    pallas_call x1, Pallas kernels, run_fused(): pl.pallas_call(lambda *refs: fused_kernel(dims, *refs), name='fused_layer...  95 us

profile of v4, /device:TPU:0, one launch (start us, length us, event | category | flops | bytes accessed | tf_op | source)
XLA Modules:
  0.0 97.8 jit_solution(14559980496006387420)
XLA Ops:
  0.6 95.0 %fused_layer.1 = (bf16[128,2048]{1,0:T(8,128)(2,1)}, bf16[128,2048]{1,0:T(8,128)(2,1)}) custom-call(bf16[128,2048]{1,0:T(8,128)(2,1)} %refs_0_.1, f32[1,2048]{1,0:T(1,128)} %bitcast.4, s32[2,128]{1,0:T(2,128)} %bitcast.5, f32[2,128]{1,0:T(2,128)} %bitcast.6, f32[1,12]{1,0:T(1,128)} %bitcast.7, f32[12,64]{1,0:T(8,128)} %refs_5_.1, f32[4,64]{1,0:T(4,128)} %refs_6_.1, ...), custom_call_target="tpu_custom_call" | custom-call | tf_op jit(solution)/shard_map/fused_layer/pallas_call | solution.py:644
  95.6 2.0 %hand_out.1 = (bf16[128,2048]{1,0:T(8,128)(2,1)}, bf16[128,2048]{1,0:T(8,128)(2,1)}) custom-call(bf16[128,2048]{1,0:T(8,128)(2,1)} %get-tuple-element.4.first_in, bf16[128,2048]{1,0:T(8,128)(2,1)} %get-tuple-element.5.second_in), custom_call_target="tpu_custom_call" | custom-call | tf_op jit(solution)/shard_map/hand_out/pallas_call | solution.py:718
